TPU v7x, 32 devices: a whole 2x2x4 slice. The times are simulated.
32 devices in a mesh: grp: 2 (over y), sp: 4 (over z), tp: 4 (over x, core).
Axes of the slice: x: 2, y: 2, z: 4, core: 2. Of those that a mesh axis runs over, the one named last changes fastest.
Arguments:
- query_rows: bfloat16 [4096, 1024], P(('grp', 'sp'), 'tp'), parts along dimension 0, may hold values from -128 to 128
- key_rows: bfloat16 [4096, 256], P(('grp', 'sp'), 'tp'), parts along dimension 0, may hold values from -4 to 4
- value_rows: bfloat16 [4096, 256], P(('grp', 'sp'), 'tp'), parts along dimension 0, may hold values from -6 to 6
- sink_logits: float32 [16], P('tp'), may hold values from 3 to 7
- residual: bfloat16 [4096, 2048], P(('grp', 'sp', 'tp')), parts along dimension 0, may hold values from -6 to 6
- out_weight: bfloat16 [1024, 2048], P('tp'), may hold values from -0.1875 to 0.1875
- norm_gain: float32 [2048], replicated, may hold values from 0.1 to 1.9
- gate_weight: bfloat16 [16, 2048, 512], P(('sp', 'tp')), may hold values from -0.125 to 0.125
- up_weight: bfloat16 [16, 2048, 512], P(('sp', 'tp')), may hold values from -0.125 to 0.125
- down_weight: bfloat16 [16, 512, 2048], P(('sp', 'tp')), may hold values from -0.25 to 0.25
- routes: int32 [4096, 2], P(('grp', 'sp', 'tp')), parts along dimension 0, may hold values from 0 to 15, as said below
- route_weight: float32 [4096, 2], P(('grp', 'sp', 'tp')), parts along dimension 0, may hold values from 0.1 to 1
Outputs:
- layer_out: bfloat16 [4096, 2048], P(('grp', 'sp', 'tp')), parts along dimension 0
There are 2 independent parts, one for each index of `grp`. A program takes and returns all parts, laid end to end along the dimension named above; an argument that names none is the same for every part. Nothing has to cross between parts.
Inputs may be any that keep to these rules, and one draw needn't show every extreme that they name: `routes`: A token's two experts differ and lie in the same group of 4 consecutive experts. Among the 128 tokens of one device (aligned blocks of 128 rows) no expert is named more than 32 times; in every block each expert of one group, the same group for all blocks, is named exactly 32 times.
All inputs are finite; a program needn't handle non-finite values.
Results may differ from a plain program's by a relative error of at most 0.013.
Values may be sent and summed in bfloat16 or wider, within the bound.
No kernel may reach another device: no remote copies, remote signals or barrier semaphores. Data moves between devices by JAX's collectives and lax.ppermute only.
A program may use at most 64 MiB of HBM per device.

v0:
```python
import jax
import jax.numpy as jnp
from jax import lax
from jax.sharding import PartitionSpec as P

HDIM = 64
WINDOW = 128


rope_base = 10000.0
norm_eps = 1e-06


def shifted(block, axis, distance):
    devices = range(lax.axis_size(axis))
    route = [(i - distance, i) for i in devices if i - distance in devices]
    return lax.ppermute(block, axis, route)


def rotate(rows, positions, heads):
    half_dim = HDIM // 2
    values = rows.astype(jnp.float32).reshape(rows.shape[0], heads, HDIM)
    inverse = rope_base ** (-jnp.arange(half_dim, dtype=jnp.float32) / half_dim)
    angles = positions.astype(jnp.float32)[:, None] * inverse[None, :]
    cosines = jnp.cos(angles)[:, None, :]
    sines = jnp.sin(angles)[:, None, :]
    lower = values[..., :half_dim]
    upper = values[..., half_dim:]
    turned = jnp.concatenate(
        [lower * cosines - upper * sines, upper * cosines + lower * sines], axis=-1
    )
    return turned.reshape(rows.shape[0], heads * HDIM).astype(jnp.bfloat16)


def per_device(
    query_rows,
    key_rows,
    value_rows,
    sink_logits,
    residual,
    out_weight,
    norm_gain,
    gate_weight,
    up_weight,
    down_weight,
    routes,
    route_weight,
):
    tok_count = query_rows.shape[0]
    head_local = query_rows.shape[1] // HDIM
    group_local = key_rows.shape[1] // HDIM
    repeat = head_local // group_local
    first_pos = lax.axis_index("sp") * tok_count
    positions = first_pos + jnp.arange(tok_count, dtype=jnp.int32)
    rot_q = rotate(query_rows, positions, head_local)
    rot_k = rotate(key_rows, positions, group_local)
    tails = jnp.stack([rot_k[tok_count - WINDOW :], value_rows[tok_count - WINDOW :]])
    earlier = shifted(tails, "sp", 1)
    blocks = tok_count // WINDOW
    q_blocks = rot_q.reshape(blocks, WINDOW, group_local, repeat, HDIM)
    k_blocks = rot_k.reshape(blocks, WINDOW, group_local, HDIM)
    v_blocks = value_rows.reshape(blocks, WINDOW, group_local, HDIM)
    k_prev = jnp.concatenate(
        [earlier[0].reshape(1, WINDOW, group_local, HDIM), k_blocks[:-1]], axis=0
    )
    v_prev = jnp.concatenate(
        [earlier[1].reshape(1, WINDOW, group_local, HDIM), v_blocks[:-1]], axis=0
    )
    k_wide = jnp.concatenate([k_prev, k_blocks], axis=1)
    v_wide = jnp.concatenate([v_prev, v_blocks], axis=1)
    query_pos = jnp.arange(WINDOW) + WINDOW
    key_pos = jnp.arange(2 * WINDOW)
    distance = query_pos[:, None] - key_pos[None, :]
    in_band = (distance >= 0) & (distance < WINDOW)
    key_global = (
        first_pos + jnp.arange(blocks)[:, None, None] * WINDOW + key_pos[None, None, :] - WINDOW
    )
    allowed = in_band[None] & (key_global >= 0)
    scores = jnp.einsum(
        "nqgrd,nkgd->grnqk", q_blocks, k_wide, preferred_element_type=jnp.float32
    ) * HDIM ** (-0.5)
    scores = jnp.where(allowed[None, None], scores, -jnp.inf)
    sink_here = sink_logits.reshape(group_local, repeat)[:, :, None, None, None]
    largest = jnp.maximum(scores.max(axis=-1, keepdims=True), sink_here)
    exp_scores = jnp.exp(scores - largest)
    denominator = exp_scores.sum(axis=-1, keepdims=True) + jnp.exp(sink_here - largest)
    probs = (exp_scores / denominator).astype(jnp.bfloat16)
    attended = jnp.einsum("grnqk,nkgd->nqgrd", probs, v_wide, preferred_element_type=jnp.float32)
    attended = attended.astype(jnp.bfloat16).reshape(tok_count, head_local * HDIM)
    row_count = residual.shape[0]
    token_rows = lax.all_to_all(attended, "tp", split_axis=0, concat_axis=1, tiled=True)
    projected = jnp.dot(
        token_rows,
        lax.all_gather(out_weight, "tp", axis=0, tiled=True),
        preferred_element_type=jnp.float32,
    )
    stream_f = (residual.astype(jnp.float32) + projected).astype(jnp.bfloat16).astype(jnp.float32)
    normed = (
        stream_f
        * lax.rsqrt(jnp.mean(stream_f * stream_f, axis=-1, keepdims=True) + norm_eps)
        * norm_gain[None, :]
    ).astype(jnp.bfloat16)
    sp_count = lax.axis_size("sp")
    tp_count = lax.axis_size("tp")
    expert_count = sp_count * tp_count
    capacity = 4 * row_count // expert_count
    width = normed.shape[1]
    flat_expert = routes.reshape(-1)
    one_hot = (flat_expert[:, None] == jnp.arange(expert_count, dtype=jnp.int32)[None, :]).astype(
        jnp.int32
    )
    slot_rank = jnp.sum((jnp.cumsum(one_hot, axis=0) - one_hot) * one_hot, axis=1)
    slot_index = flat_expert * capacity + slot_rank
    token_of = jnp.arange(2 * row_count, dtype=jnp.int32) // 2
    outgoing = (
        jnp.zeros((expert_count * capacity, width), jnp.bfloat16)
        .at[slot_index]
        .set(normed[token_of])
    )
    outgoing = outgoing.reshape(expert_count, capacity, width)
    arrived = lax.all_to_all(outgoing, ("sp", "tp"), split_axis=0, concat_axis=0, tiled=True)
    flat_rows = arrived.reshape(-1, width)
    gate_out = jnp.dot(flat_rows, gate_weight[0], preferred_element_type=jnp.float32)
    up_out = jnp.dot(flat_rows, up_weight[0], preferred_element_type=jnp.float32)
    hidden = (jax.nn.silu(gate_out) * up_out).astype(jnp.bfloat16)
    produced = jnp.dot(hidden, down_weight[0], preferred_element_type=jnp.float32).astype(
        jnp.bfloat16
    )
    returned = lax.all_to_all(
        produced.reshape(arrived.shape), ("sp", "tp"), split_axis=0, concat_axis=0, tiled=True
    )
    gathered = returned.reshape(expert_count * capacity, width)[slot_index].astype(jnp.float32)
    weighted = gathered * route_weight.reshape(-1)[:, None]
    combined = weighted.reshape(row_count, 2, width).sum(axis=1)
    return (stream_f + combined).astype(jnp.bfloat16)


def solution(mesh):
    in_specs = (
        P(("grp", "sp"), "tp"),
        P(("grp", "sp"), "tp"),
        P(("grp", "sp"), "tp"),
        P("tp"),
        P(("grp", "sp", "tp"), None),
        P("tp", None),
        P(),
        P(("sp", "tp"), None, None),
        P(("sp", "tp"), None, None),
        P(("sp", "tp"), None, None),
        P(("grp", "sp", "tp"), None),
        P(("grp", "sp", "tp"), None),
    )
    out_specs = P(("grp", "sp", "tp"), None)
    return jax.shard_map(
        per_device, mesh=mesh, in_specs=in_specs, out_specs=out_specs, check_vma=False
    )
```

profile of v0, /device:TPU:11, one launch (start us, length us, event | category | flops | bytes accessed | tf_op | source)
XLA Modules:
  0.0 195.3 jit_solution(5464959872850920019)
XLA Ops:
  6.5 0.0 copy-start
  6.5 0.0 copy-start.5
  6.5 0.0 copy-start.2
  6.5 0.0 all-gather.2.cloned.1.call-start
  6.5 0.7 all-gather.2.cloned.1.call-update
  7.3 0.0 copy-start.3
  7.3 0.0 slice-start
  7.3 0.9 bitcast_convert_fusion
  8.2 0.3 fusion.38
  8.5 0.7 slice_bitcast_fusion.4
  9.3 3.2 %collective-permute-start = (bf16[2,128,64]{1,2,0:T(8,128)(2,1)S(1)}, bf16[2,128,64]{1,2,0:T(8,128)(2,1)S(1)}, u32[]{:S(2)}, u32[]{:S(2)}) collective-permute-start(bf16[2,128,64]{1,2,0:T(8,128)(2,1)S(1)} %pad_maximum_fusion), channel_id=1, source_target_pairs={{0,4},{4,8},{8,12},{1,5},{5,9},{9,13},{2,6},{6,10},{10,14},{3,7},{... | collective-permute-start | bytes 98312 | tf_op jit(solution)/shard_map/ppermute | solution.py:17
  12.5 0.8 copy.25
  13.2 0.1 eq.29
  13.4 0.1 eq.25
  13.5 0.0 copy-done.2
  13.5 0.1 copy.21
  13.7 0.1 convert.12
  13.8 0.6 reduce-window.6
  14.3 0.2 slice_reduce_fusion
  14.6 0.1 fusion.42
  14.7 0.1 add_compare_fusion
  14.8 0.0 copy-done.5
  14.8 0.3 multiply_cosine_fusion
  15.2 0.2 broadcast_and_fusion
  15.4 0.1 subtract_convert_fusion
  15.5 0.0 copy-start.6
  15.5 0.0 copy-done.3
  15.5 0.0 slice-done
  15.6 0.1 copy.24
  15.7 0.1 mul.180
  15.8 0.0 collective-permute-done
  15.9 0.5 fusion.47
  16.4 0.0 copy-done.6
  16.4 0.1 broadcast_maximum_fusion
  16.5 0.3 fusion.7
  16.8 0.1 exponential_add_fusion
  16.9 1.2 convolution_convert_fusion.1
  18.1 4.5 %all-to-all-start = ((bf16[4,128,256]{1,2,0:T(8,128)(2,1)}), bf16[4,128,256]{1,2,0:T(8,128)(2,1)S(1)}, u32[]{:S(2)}, u32[]{:S(2)}) async-start(bf16[4,128,256]{1,2,0:T(8,128)(2,1)} %bitcast.20), calls=%async_computation | async-start | bytes 524288 | tf_op jit(solution)/shard_map/all_to_all | solution.py:91
  22.5 7.4 %all-to-all-done = bf16[4,128,256]{1,2,0:T(8,128)(2,1)S(1)} async-done(((bf16[4,128,256]{1,2,0:T(8,128)(2,1)}), bf16[4,128,256]{1,2,0:T(8,128)(2,1)S(1)}, u32[]{:S(2)}, u32[]{:S(2)}) %all-to-all-start) | async-done | bytes 262176 | tf_op jit(solution)/shard_map/all_to_all | solution.py:91
  29.9 16.9 %all-gather.2.cloned.1.call-done = bf16[1024,2048]{1,0:T(8,128)(2,1)} async-done(((bf16[256,2048]{1,0:T(8,128)(2,1)}), bf16[1024,2048]{1,0:T(8,128)(2,1)}) %all-gather.2.cloned.1.call-update) | async-done | bytes 4194320 | tf_op jit(solution)/shard_map/all_gather | solution.py:94
  46.9 0.0 copy-start.4
  46.9 3.1 %multiply_reduce_fusion.1 = (f32[128]{0:T(128)S(1)}, f32[128,2048]{1,0:T(8,128)S(1)}) fusion(bf16[128,1024]{0,1:T(8,128)(2,1)S(1)} %bitcast.116, bf16[1024,2048]{1,0:T(8,128)(2,1)} %all-gather.2.cloned.1.call-done, bf16[128,2048]{1,0:T(8,128)(2,1)} %param.16), kind=kOutput, calls=%fused_computation.25 | convolution fusion | flops 538443648 | bytes 6029824 | tf_op jit(solution)/shard_map/dot_general | solution.py:92
  50.0 0.0 copy-done.4
  50.0 1.0 multiply_convert_fusion
  51.0 7.3 %scatter_custom_fusion = bf16[512,2048]{1,0:T(8,128)(2,1)} fusion(s32[256]{0:T(256)S(1)} %bitcast.119, bf16[128,2048]{1,0:T(8,128)(2,1)} %multiply_convert_fusion, s32[1024]{0:T(1024)S(1)} %pad_clamp_fusion.1, bf16[]{:T(256)} %constant.56.clone.1), kind=kCustom, calls=%fused_computation.21 | custom fusion | bytes 2097664 | tf_op jit(solution)/shard_map/scatter | solution.py:118
  58.3 0.0 copy-start.8
  58.3 53.3 %all_to_all.29 = bf16[16,32,2048]{2,1,0:T(8,128)(2,1)S(1)} all-to-all(bf16[16,32,2048]{2,1,0:T(8,128)(2,1)} %bitcast.112), channel_id=1, replica_groups=mesh['grp'=2,'sp'=4,'tp'=4] {'sp','tp'}, dimensions={0} | all-to-all | bytes 4194304 | tf_op jit(solution)/shard_map/all_to_all | solution.py:121
  111.6 0.0 copy-start.1
  111.7 1.3 copy-done.1
  112.9 0.0 copy-done.8
  112.9 2.2 %fusion.5 = f32[512,512]{1,0:T(8,128)} fusion(bf16[512,2048]{1,0:T(8,128)(2,1)S(1)} %bitcast.114, bf16[1,2048,512]{2,1,0:T(8,128)(2,1)S(1)} %copy-done.8), kind=kOutput, calls=%fused_computation.11 | convolution fusion | flops 1073741824 | bytes 5242880 | tf_op jit(solution)/shard_map/dot_general | solution.py:123
  115.2 0.0 copy-done
  115.2 6.3 %convolution_convert_fusion = bf16[512,2048]{1,0:T(8,128)(2,1)} fusion(bf16[1,512,2048]{2,1,0:T(8,128)(2,1)S(1)} %copy-done, bf16[512,2048]{1,0:T(8,128)(2,1)} %bitcast.115, bf16[1,2048,512]{2,1,0:T(8,128)(2,1)} %param.20, f32[512,512]{1,0:T(8,128)} %fusion.5), kind=kOutput, calls=%fused_computation.3 | convolution fusion | flops 2150105088 | bytes 9437184 | tf_op jit(solution)/shard_map/dot_general | solution.py:126
  121.5 0.0 copy-start.7
  121.5 5.1 %all-to-all-start.2 = ((bf16[16,32,2048]{2,1,0:T(8,128)(2,1)}), bf16[16,32,2048]{2,1,0:T(8,128)(2,1)}, u32[]{:S(2)}, u32[]{:S(2)}) async-start(bf16[16,32,2048]{2,1,0:T(8,128)(2,1)} %bitcast.113), calls=%async_computation.2 | async-start | bytes 4194304 | tf_op jit(solution)/shard_map/all_to_all | solution.py:129
  126.6 0.0 copy-done.7
  126.6 0.1 copy.28
  126.7 47.4 %all-to-all-done.2 = bf16[16,32,2048]{2,1,0:T(8,128)(2,1)} async-done(((bf16[16,32,2048]{2,1,0:T(8,128)(2,1)}), bf16[16,32,2048]{2,1,0:T(8,128)(2,1)}, u32[]{:S(2)}, u32[]{:S(2)}) %all-to-all-start.2) | async-done | bytes 2097184 | tf_op jit(solution)/shard_map/all_to_all | solution.py:129
  174.1 5.2 %gather_fusion = bf16[256,2048]{1,0:T(8,128)(2,1)} fusion(bf16[512,2048]{1,0:T(8,128)(2,1)} %bitcast.33, s32[1024]{0:T(1024)S(1)} %pad_clamp_fusion), kind=kCustom, calls=%fused_computation.1 | custom fusion | bytes 2098176 | tf_op jit(solution)/shard_map/gather | solution.py:132
  179.3 3.4 %reshape.391 = f32[128,2,2048]{2,1,0:T(2,128)} reshape(bf16[256,2048]{1,0:T(8,128)(2,1)} %gather_fusion) | data formatting | bytes 3145728 | tf_op jit(solution)/shard_map/convert_element_type | solution.py:132
  182.7 4.8 %multiply_reduce_fusion = f32[128,2048]{1,0:T(8,128)S(1)} fusion(f32[128,2,2048]{2,1,0:T(2,128)} %reshape.391, f32[128,2]{1,0:T(8,128)S(1)} %copy.28), kind=kLoop, calls=%fused_computation.13 | loop fusion | flops 786432 | bytes 3146752 | tf_op jit(solution)/shard_map/reduce_sum | solution.py:134
  187.5 0.9 add_convert_fusion
  (24 shorter events, 0.3 us)
Async XLA Ops:
  6.5 108.6 %copy-start = (bf16[1,512,2048]{2,1,0:T(8,128)(2,1)S(1)}, bf16[1,512,2048]{2,1,0:T(8,128)(2,1)}, u32[]{:S(2)}) copy-start(bf16[1,512,2048]{2,1,0:T(8,128)(2,1)} %param.21) | copy-start | bytes 6291460
  6.5 8.2 %copy-start.5 = (s32[128,2]{0,1:T(2,128)S(1)}, s32[128,2]{0,1:T(2,128)}, u32[]{:S(2)}) copy-start(s32[128,2]{0,1:T(2,128)} %param.22) | copy-start | bytes 3076
  6.5 7.0 %copy-start.2 = (bf16[512,256]{1,0:T(8,128)(2,1)S(1)}, bf16[512,256]{1,0:T(8,128)(2,1)}, u32[]{:S(2)}) copy-start(bf16[512,256]{1,0:T(8,128)(2,1)} %param.12) | copy-start | bytes 786436
  6.5 40.3 %all-gather.2.cloned.1.call-start = ((), (), s32[]{:S(2)}) async-start(), calls=%async_computation.3 | async-start | bytes 5242880 | tf_op jit(solution)/shard_map/all_gather | solution.py:94
  7.3 8.2 %copy-start.3 = (bf16[512,64]{0,1:T(8,128)(2,1)S(1)}, bf16[512,64]{0,1:T(8,128)(2,1)}, u32[]{:S(2)}) copy-start(bf16[512,64]{0,1:T(8,128)(2,1)} %param.14) | copy-start | bytes 196612
  7.3 8.2 %slice-start = ((bf16[512,64]{0,1:T(8,128)(2,1)}), bf16[384,64]{0,1:T(8,128)(2,1)S(1)}, s32[]{:S(2)}) async-start(bf16[512,64]{0,1:T(8,128)(2,1)} %param.14), calls=%async_computation.4 | async-start | bytes 98304 | tf_op jit(solution)/shard_map/slice | solution.py:67
  9.3 6.6 %collective-permute-start = (bf16[2,128,64]{1,2,0:T(8,128)(2,1)S(1)}, bf16[2,128,64]{1,2,0:T(8,128)(2,1)S(1)}, u32[]{:S(2)}, u32[]{:S(2)}) collective-permute-start(bf16[2,128,64]{1,2,0:T(8,128)(2,1)S(1)} %pad_maximum_fusion), channel_id=1, source_target_pairs={{0,4},{4,8},{8,12},{1,5},{5,9},{9,13},{2,6},{6,10},{10,14},{3,7},{... | collective-permute-start | bytes 98312 | tf_op jit(solution)/shard_map/ppermute | solution.py:17
  15.5 0.9 copy-start.6
  18.1 11.8 %all-to-all-start = ((bf16[4,128,256]{1,2,0:T(8,128)(2,1)}), bf16[4,128,256]{1,2,0:T(8,128)(2,1)S(1)}, u32[]{:S(2)}, u32[]{:S(2)}) async-start(bf16[4,128,256]{1,2,0:T(8,128)(2,1)} %bitcast.20), calls=%async_computation | async-start | bytes 524288 | tf_op jit(solution)/shard_map/all_to_all | solution.py:91
  46.9 3.2 %copy-start.4 = (f32[2048]{0:T(1024)S(1)}, f32[2048]{0:T(1024)}, u32[]{:S(2)}) copy-start(f32[2048]{0:T(1024)} %param.18) | copy-start | bytes 24580
  58.3 54.6 %copy-start.8 = (bf16[1,2048,512]{2,1,0:T(8,128)(2,1)S(1)}, bf16[1,2048,512]{2,1,0:T(8,128)(2,1)}, u32[]{:S(2)}) copy-start(bf16[1,2048,512]{2,1,0:T(8,128)(2,1)} %param.19) | copy-start | bytes 6291460
  111.6 1.3 copy-start.1
  121.5 5.1 %copy-start.7 = (f32[128,2]{0,1:T(2,128)S(1)}, f32[128,2]{0,1:T(2,128)}, u32[]{:S(2)}) copy-start(f32[128,2]{0,1:T(2,128)} %param.23) | copy-start | bytes 3076
  121.5 52.7 %all-to-all-start.2 = ((bf16[16,32,2048]{2,1,0:T(8,128)(2,1)}), bf16[16,32,2048]{2,1,0:T(8,128)(2,1)}, u32[]{:S(2)}, u32[]{:S(2)}) async-start(bf16[16,32,2048]{2,1,0:T(8,128)(2,1)} %bitcast.113), calls=%async_computation.2 | async-start | bytes 4194304 | tf_op jit(solution)/shard_map/all_to_all | solution.py:129
Sparse Core Ops, SparseCore 0:
  8.9 37.9 all-gather.1
where the time goes:
time: 196 us; the launch traced here: 195 us
  waiting for transfers between devices  72.4 us (37%)
  blocking collectives  53.3 us (27%)
  local copies, waits for them, and re-layouts  19.8 us (10%)
  between operations  13.7 us (7%)
  matrix products  13.4 us (7%)
  starting transfers between devices  12.8 us (7%)
  other arithmetic  9.91 us (5%)
    all_to_all x1, blocking collectives, per_device(): lax.all_to_all(outgoing, ('sp', 'tp'), split_axis=0, concat_axis=0, tiled...  53.3 us
    all_to_all x1, waiting for transfers between devices, per_device(): lax.all_to_all(produced.reshape(arrived.shape), ('sp', 'tp'), split_axis=...  47.4 us
    all_gather x1, waiting for transfers between devices, per_device(): lax.all_gather(out_weight, 'tp', axis=0, tiled=True)  16.9 us
    all_to_all x1, waiting for transfers between devices, per_device(): lax.all_to_all(attended, 'tp', split_axis=0, concat_axis=1, tiled=True)  7.37 us
    scatter x1, local copies, waits for them, and re-layouts, per_device(): outgoing = jnp.zeros((expert_count * capacity, width), jnp.bfloat16).at[s...  7.33 us
    dot_general x1, matrix products, per_device(): jnp.dot(hidden, down_weight[0], preferred_element_type=jnp.float32)  6.28 us
    gather x1, local copies, waits for them, and re-layouts, per_device(): returned.reshape(expert_count * capacity, width)[slot_index]  5.2 us
    all_to_all x1, starting transfers between devices, per_device(): lax.all_to_all(produced.reshape(arrived.shape), ('sp', 'tp'), split_axis=...  5.14 us
  transfers between devices with their start and end apart: 4, of which 3 were waited for; matrix products, arithmetic and copies ran while one was open for 4% of the time, Pallas kernels for 0%

commit v1 on v0

--- a/solution.py
+++ b/solution.py
@@ -15,6 +15,31 @@
     devices = range(lax.axis_size(axis))
     route = [(i - distance, i) for i in devices if i - distance in devices]
     return lax.ppermute(block, axis, route)
+
+
+def swapped(block, axis, offset):
+    return lax.ppermute(block, axis, [(i, i ^ offset) for i in range(lax.axis_size(axis))])
+
+
+def gathered_by_doubling(block, axis):
+    blocks = {0: block}
+    offset = lax.axis_size(axis) // 2
+    while offset:
+        blocks.update({m ^ offset: swapped(b, axis, offset) for m, b in blocks.items()})
+        offset //= 2
+    return blocks
+
+
+def slots_of(routes, expert_count, capacity):
+    count = routes.shape[0]
+    experts = jnp.arange(expert_count, dtype=jnp.int32)
+    named = (routes[:, :, None] == experts[None, None, :]).astype(jnp.bfloat16)
+    either = named[:, 0] + named[:, 1]
+    row = jnp.arange(count, dtype=jnp.int32)
+    earlier = (row[:, None] > row[None, :]).astype(jnp.bfloat16)
+    before = jnp.dot(earlier, either, preferred_element_type=jnp.float32)
+    rank = jnp.sum(before[:, None, :] * named.astype(jnp.float32), axis=-1).astype(jnp.int32)
+    return routes * capacity + rank
 
 
 def rotate(rows, positions, heads):
@@ -46,6 +71,7 @@
     routes,
     route_weight,
 ):
+    weight_of = gathered_by_doubling(out_weight, "tp")
     tok_count = query_rows.shape[0]
     head_local = query_rows.shape[1] // HDIM
     group_local = key_rows.shape[1] // HDIM
@@ -88,12 +114,15 @@
     attended = jnp.einsum("grnqk,nkgd->nqgrd", probs, v_wide, preferred_element_type=jnp.float32)
     attended = attended.astype(jnp.bfloat16).reshape(tok_count, head_local * HDIM)
     row_count = residual.shape[0]
+    heads_wide = attended.shape[1]
     token_rows = lax.all_to_all(attended, "tp", split_axis=0, concat_axis=1, tiled=True)
-    projected = jnp.dot(
-        token_rows,
-        lax.all_gather(out_weight, "tp", axis=0, tiled=True),
-        preferred_element_type=jnp.float32,
-    )
+    here = lax.axis_index("tp")
+    projected = 0.0
+    for offset in sorted(weight_of):
+        part = lax.dynamic_slice_in_dim(token_rows, (here ^ offset) * heads_wide, heads_wide, 1)
+        projected = projected + jnp.dot(
+            part, weight_of[offset], preferred_element_type=jnp.float32
+        )
     stream_f = (residual.astype(jnp.float32) + projected).astype(jnp.bfloat16).astype(jnp.float32)
     normed = (
         stream_f
@@ -105,18 +134,12 @@
     expert_count = sp_count * tp_count
     capacity = 4 * row_count // expert_count
     width = normed.shape[1]
-    flat_expert = routes.reshape(-1)
-    one_hot = (flat_expert[:, None] == jnp.arange(expert_count, dtype=jnp.int32)[None, :]).astype(
-        jnp.int32
-    )
-    slot_rank = jnp.sum((jnp.cumsum(one_hot, axis=0) - one_hot) * one_hot, axis=1)
-    slot_index = flat_expert * capacity + slot_rank
-    token_of = jnp.arange(2 * row_count, dtype=jnp.int32) // 2
-    outgoing = (
-        jnp.zeros((expert_count * capacity, width), jnp.bfloat16)
-        .at[slot_index]
-        .set(normed[token_of])
-    )
+    slot_index = slots_of(routes, expert_count, capacity)
+    slot_ids = jnp.arange(expert_count * capacity, dtype=jnp.int32)
+    place = (slot_index[:, :, None] == slot_ids[None, None, :]).astype(jnp.bfloat16)
+    outgoing = jnp.einsum(
+        "ns,nd->sd", place[:, 0] + place[:, 1], normed, preferred_element_type=jnp.float32
+    ).astype(jnp.bfloat16)
     outgoing = outgoing.reshape(expert_count, capacity, width)
     arrived = lax.all_to_all(outgoing, ("sp", "tp"), split_axis=0, concat_axis=0, tiled=True)
     flat_rows = arrived.reshape(-1, width)
@@ -129,10 +152,12 @@
     returned = lax.all_to_all(
         produced.reshape(arrived.shape), ("sp", "tp"), split_axis=0, concat_axis=0, tiled=True
     )
-    gathered = returned.reshape(expert_count * capacity, width)[slot_index].astype(jnp.float32)
-    weighted = gathered * route_weight.reshape(-1)[:, None]
-    combined = weighted.reshape(row_count, 2, width).sum(axis=1)
-    return (stream_f + combined).astype(jnp.bfloat16)
+    returned = returned.reshape(expert_count * capacity, width)
+    total = stream_f
+    for k in range(2):
+        picked = jnp.dot(place[:, k], returned, preferred_element_type=jnp.float32)
+        total = total + picked * route_weight[:, k : k + 1]
+    return total.astype(jnp.bfloat16)
 
 
 def solution(mesh):

time: 196 us -> 157 us (0.80)
  local copies, waits for them, and re-layouts: 19.8 us -> 3.28 us
  waiting for transfers between devices: 72.4 us -> 57.8 us
  between operations: 13.7 us -> 0.38 us
  matrix products: 13.4 us -> 21.3 us
  other arithmetic: 9.91 us -> 3.37 us
  starting transfers between devices: 12.8 us -> 15.9 us
    all_gather x1 -> x0, waiting for transfers between devices: 16.9 us -> none  [per_device(): lax.all_gather(out_weight, 'tp', axis=0, tiled=True)]
    ppermute x0 -> x3, waiting for transfers between devices: none -> 9.88 us  [swapped(): lax.ppermute(block, axis, [(i, i ^ offset) for i in range(lax.axis_size(a...]
    dot_general x1 -> x8, matrix products: 3.13 us -> 11.1 us  [the longest x4 5.24 us: per_device(): jnp.dot(part, weight_of[offset], preferred_element_type=jnp.float32)]
    scatter x1 -> x0, local copies, waits for them, and re-layouts: 7.33 us -> none  [per_device(): outgoing = jnp.zeros((expert_count * capacity, width), jnp.bfloat16).at[s...]
    all_to_all x1, waiting for transfers between devices: 7.37 us -> 0.36 us  [per_device(): lax.all_to_all(attended, 'tp', split_axis=0, concat_axis=1, tiled=True)]
    gather x1 -> x0, local copies, waits for them, and re-layouts: 5.2 us -> none  [per_device(): returned.reshape(expert_count * capacity, width)[slot_index]]
    reduce_sum x2 -> x1, other arithmetic: 4.9 us -> 0.03 us  [slots_of(): jnp.sum(before[:, None, :] * named.astype(jnp.float32), axis=-1)]
    convert_element_type x1 -> x0, local copies, waits for them, and re-layouts: 3.39 us -> none  [per_device(): returned.reshape(expert_count * capacity, width)[slot_index]]
  transfers between devices with their start and end apart: 4 -> 6, of which waited for: 3 -> 3; matrix products, arithmetic and copies ran while one was open for 4% -> 7% of each run, Pallas kernels for 0% -> 0%
where the time goes in v1:
time: 157 us; the launch traced here: 156 us
  waiting for transfers between devices  57.8 us (37%)
  blocking collectives  54 us (34%)
  matrix products  21.3 us (14%)
  starting transfers between devices  15.9 us (10%)
  other arithmetic  3.37 us (2%)
  local copies, waits for them, and re-layouts  3.28 us (2%)
    all_to_all x1, blocking collectives, per_device(): lax.all_to_all(outgoing, ('sp', 'tp'), split_axis=0, concat_axis=0, tiled...  54 us
    all_to_all x1, waiting for transfers between devices, per_device(): lax.all_to_all(produced.reshape(arrived.shape), ('sp', 'tp'), split_axis=...  47.5 us
    ppermute x3, waiting for transfers between devices, swapped(): lax.ppermute(block, axis, [(i, i ^ offset) for i in range(lax.axis_size(a...  9.88 us
    dot_general x1, matrix products, per_device(): jnp.dot(hidden, down_weight[0], preferred_element_type=jnp.float32)  6.26 us
    dot_general x4, matrix products, per_device(): jnp.dot(part, weight_of[offset], preferred_element_type=jnp.float32)  5.24 us
    all_to_all x1, starting transfers between devices, per_device(): lax.all_to_all(produced.reshape(arrived.shape), ('sp', 'tp'), split_axis=...  5.16 us
    all_to_all x1, starting transfers between devices, per_device(): lax.all_to_all(attended, 'tp', split_axis=0, concat_axis=1, tiled=True)  5.12 us
    dot_general x2, matrix products, per_device(): picked = jnp.dot(place[:, k], returned, preferred_element_type=jnp.float32)  4.94 us
  transfers between devices with their start and end apart: 6, of which 3 were waited for; matrix products, arithmetic and copies ran while one was open for 7% of the time, Pallas kernels for 0%

profile of v1, /device:TPU:11, one launch (start us, length us, event | category | flops | bytes accessed | tf_op | source)
XLA Modules:
  0.0 156.0 jit_solution(10874022914395107994)
XLA Ops:
  0.0 0.0 copy-start
  0.0 0.0 copy-start.5
  0.0 0.0 slice-start
  0.0 0.0 copy-start.6
  0.0 0.7 collective-permute-start.1
  0.8 0.3 collective-permute-start.2
  1.0 0.9 bitcast_convert_fusion
  1.9 0.3 fusion.44
  2.2 0.7 slice_bitcast_fusion.8
  3.0 3.2 %collective-permute-start = (bf16[2,128,64]{1,2,0:T(8,128)(2,1)S(1)}, bf16[2,128,64]{1,2,0:T(8,128)(2,1)S(1)}, u32[]{:S(2)}, u32[]{:S(2)}) collective-permute-start(bf16[2,128,64]{1,2,0:T(8,128)(2,1)S(1)} %pad_maximum_fusion), channel_id=1, source_target_pairs={{0,4},{4,8},{8,12},{1,5},{5,9},{9,13},{2,6},{6,10},{10,14},{3,7},{... | collective-permute-start | bytes 98312 | tf_op jit(solution)/shard_map/ppermute | solution.py:17
  6.2 0.3 multiply_cosine_fusion
  6.5 1.1 copy.23
  7.6 0.1 convert.11
  7.7 0.1 add_compare_fusion
  7.8 0.0 copy-done.6
  7.8 0.1 fusion.51
  8.0 0.2 broadcast_and_fusion
  8.2 0.1 subtract_convert_fusion
  8.3 0.0 copy-start.8
  8.3 0.0 copy-done.5
  8.4 0.0 slice-done
  8.5 0.0 collective-permute-done
  8.5 0.5 fusion.64
  9.0 0.0 copy-done.8
  9.0 0.1 broadcast_maximum_fusion
  9.1 0.3 fusion.11
  9.4 0.1 exponential_add_fusion
  9.5 0.0 copy-start.2
  9.5 1.2 convolution_convert_fusion.2
  10.7 5.1 %all-to-all-start = ((bf16[4,128,256]{1,2,0:T(8,128)(2,1)}), bf16[4,128,256]{1,2,0:T(8,128)(2,1)S(1)}, u32[]{:S(2)}, u32[]{:S(2)}) async-start(bf16[4,128,256]{1,2,0:T(8,128)(2,1)} %bitcast.119), calls=%async_computation | async-start | bytes 524288 | tf_op jit(solution)/shard_map/all_to_all | solution.py:118
  15.8 9.9 %collective-permute-done.2 = bf16[256,2048]{1,0:T(8,128)(2,1)} collective-permute-done((bf16[256,2048]{1,0:T(8,128)(2,1)}, bf16[256,2048]{1,0:T(8,128)(2,1)}, u32[]{:S(2)}, u32[]{:S(2)}) %collective-permute-start.2) | collective-permute-done | bytes 1048608 | tf_op jit(solution)/shard_map/ppermute | solution.py:21
  25.7 1.5 collective-permute-start.3
  27.2 0.9 iota_compare_fusion
  28.1 0.4 all-to-all-done
  28.4 0.0 copy-done.2
  28.4 0.3 fusion.49
  28.8 0.0 collective-permute-done.1
  28.8 1.6 %convolution_add_fusion.2 = f32[128,2048]{1,0:T(8,128)S(1)} fusion(f32[128,2048]{1,0:T(8,128)S(1)} %fusion.49, bf16[256,2048]{1,0:T(8,128)(2,1)} %collective-permute-done.1, bf16[128,1024]{0,1:T(8,128)(2,1)S(1)} %bitcast.115, s32[]{:T(128)S(6)} %select_n.18), kind=kOutput, calls=%fused_computation.9 | convolution fusion | flops 134479872 | bytes 3211268 | tf_op jit(solution)/shard_map/dot_general | solution.py:123
  30.3 0.0 copy-start.4
  30.4 1.6 %convolution_add_fusion.1 = f32[128,2048]{1,0:T(8,128)S(1)} fusion(f32[128,2048]{1,0:T(8,128)S(1)} %convolution_add_fusion.2, bf16[256,2048]{1,0:T(8,128)(2,1)} %collective-permute-done.2, bf16[128,1024]{0,1:T(8,128)(2,1)S(1)} %bitcast.116, s32[]{:T(128)S(6)} %select_n.19), kind=kOutput, calls=%fused_computation.8 | convolution fusion | flops 134479872 | bytes 3211268 | tf_op jit(solution)/shard_map/dot_general | solution.py:123
  32.0 0.0 copy-start.3
  32.0 0.0 copy-start.7
  32.0 0.0 collective-permute-done.3
  32.0 0.0 copy-done.4
  32.0 1.7 %multiply_reduce_fusion = (f32[128]{0:T(128)S(1)}, f32[128,2048]{1,0:T(8,128)S(1)}) fusion(f32[128,2048]{1,0:T(8,128)S(1)} %convolution_add_fusion.1, bf16[256,2048]{1,0:T(8,128)(2,1)} %collective-permute-done.3, bf16[128,1024]{0,1:T(8,128)(2,1)S(1)} %bitcast.117, s32[]{:T(128)S(6)} %select_n.20, bf16[128,2048]{1,0:T(8,128)(2,1)S(1)} %copy-done.4), kind=kOutput, calls=%fused_computation.27 | convolution fusion | flops 136052608 | bytes 3736068 | tf_op jit(solution)/shard_map/dot_general | solution.py:123
  33.8 0.0 copy-done.3
  33.8 0.0 copy-done.7
  33.8 0.8 convolution_convert_fusion
  34.6 0.0 copy-start.10
  34.6 54.0 %all_to_all.29 = bf16[16,32,2048]{2,1,0:T(8,128)(2,1)S(1)} all-to-all(bf16[16,32,2048]{2,1,0:T(8,128)(2,1)S(1)} %bitcast.110), channel_id=1, replica_groups=mesh['grp'=2,'sp'=4,'tp'=4] {'sp','tp'}, dimensions={0} | all-to-all | bytes 4194304 | tf_op jit(solution)/shard_map/all_to_all | solution.py:144
  88.6 0.0 copy-start.1
  88.6 1.3 copy-done.1
  89.9 0.0 copy-done.10
  89.9 2.3 %fusion.9 = f32[512,512]{1,0:T(8,128)} fusion(bf16[512,2048]{1,0:T(8,128)(2,1)S(1)} %bitcast.112, bf16[1,2048,512]{2,1,0:T(8,128)(2,1)S(1)} %copy-done.10), kind=kOutput, calls=%fused_computation.17 | convolution fusion | flops 1073741824 | bytes 5242880 | tf_op jit(solution)/shard_map/dot_general | solution.py:146
  92.1 0.0 copy-done
  92.1 6.3 %convolution_convert_fusion.1 = bf16[512,2048]{1,0:T(8,128)(2,1)} fusion(bf16[1,512,2048]{2,1,0:T(8,128)(2,1)S(1)} %copy-done, bf16[512,2048]{1,0:T(8,128)(2,1)} %bitcast.113, bf16[1,2048,512]{2,1,0:T(8,128)(2,1)} %param.20, f32[512,512]{1,0:T(8,128)} %fusion.9), kind=kOutput, calls=%fused_computation.1 | convolution fusion | flops 2150105088 | bytes 9437184 | tf_op jit(solution)/shard_map/dot_general | solution.py:149
  98.4 0.0 copy-start.9
  98.4 5.2 %all-to-all-start.2 = ((bf16[16,32,2048]{2,1,0:T(8,128)(2,1)}), bf16[16,32,2048]{2,1,0:T(8,128)(2,1)}, u32[]{:S(2)}, u32[]{:S(2)}) async-start(bf16[16,32,2048]{2,1,0:T(8,128)(2,1)} %bitcast.111), calls=%async_computation.2 | async-start | bytes 4194304 | tf_op jit(solution)/shard_map/all_to_all | solution.py:152
  103.6 0.0 copy-done.9
  103.6 47.5 %all-to-all-done.2 = bf16[16,32,2048]{2,1,0:T(8,128)(2,1)} async-done(((bf16[16,32,2048]{2,1,0:T(8,128)(2,1)}), bf16[16,32,2048]{2,1,0:T(8,128)(2,1)}, u32[]{:S(2)}, u32[]{:S(2)}) %all-to-all-start.2) | async-done | bytes 2097184 | tf_op jit(solution)/shard_map/all_to_all | solution.py:152
  151.1 2.1 %fusion.1 = f32[128,2048]{1,0:T(8,128)S(1)} fusion(f32[128,2048]{1,0:T(8,128)S(1)} %get-tuple-element.20, bf16[512,2048]{1,0:T(8,128)(2,1)} %bitcast.33, f32[128]{0:T(128)S(1)} %get-tuple-element.14, pred[128,2,512]{2,0,1:T(32,128)(4,1)S(1)} %get-tuple-element.15), kind=kOutput, calls=%fused_computation.5 | convolution fusion | flops 268959744 | bytes 4260352 | tf_op jit(solution)/shard_map/dot_general | solution.py:158
  153.2 2.9 %fusion.5 = bf16[128,2048]{1,0:T(8,128)(2,1)} fusion(f32[128,2048]{1,0:T(8,128)S(1)} %fusion.1, bf16[512,2048]{1,0:T(8,128)(2,1)} %bitcast.33, f32[128]{0:T(128)S(1)} %get-tuple-element.13, pred[128,2,512]{2,0,1:T(32,128)(4,1)S(1)} %get-tuple-element.15), kind=kOutput, calls=%fused_computation.12 | convolution fusion | flops 269221888 | bytes 3736064 | tf_op jit(solution)/shard_map/dot_general | solution.py:158
  (20 shorter events, 0.2 us)
Async XLA Ops:
  0.0 92.1 %copy-start = (bf16[1,512,2048]{2,1,0:T(8,128)(2,1)S(1)}, bf16[1,512,2048]{2,1,0:T(8,128)(2,1)}, u32[]{:S(2)}) copy-start(bf16[1,512,2048]{2,1,0:T(8,128)(2,1)} %param.21) | copy-start | bytes 6291460
  0.0 8.3 %copy-start.5 = (bf16[512,64]{0,1:T(8,128)(2,1)S(1)}, bf16[512,64]{0,1:T(8,128)(2,1)}, u32[]{:S(2)}) copy-start(bf16[512,64]{0,1:T(8,128)(2,1)} %param.14) | copy-start | bytes 196612
  0.0 8.4 %slice-start = ((bf16[512,64]{0,1:T(8,128)(2,1)}), bf16[384,64]{0,1:T(8,128)(2,1)S(1)}, s32[]{:S(2)}) async-start(bf16[512,64]{0,1:T(8,128)(2,1)} %param.14), calls=%async_computation.3 | async-start | bytes 98304 | tf_op jit(solution)/shard_map/slice | solution.py:93
  0.0 7.8 %copy-start.6 = (s32[128,2]{0,1:T(2,128)S(1)}, s32[128,2]{0,1:T(2,128)}, u32[]{:S(2)}) copy-start(s32[128,2]{0,1:T(2,128)} %param.22) | copy-start | bytes 3076
  0.0 28.7 %collective-permute-start.1 = (bf16[256,2048]{1,0:T(8,128)(2,1)}, bf16[256,2048]{1,0:T(8,128)(2,1)}, u32[]{:S(2)}, u32[]{:S(2)}) collective-permute-start(bf16[256,2048]{1,0:T(8,128)(2,1)} %param.17), channel_id=1, source_target_pairs={{0,1},{1,0},{2,3},{3,2},{4,5},{5,4},{6,7},{7,6},{8,9},{9,8},{10,11... | collective-permute-start | bytes 3145736 | tf_op jit(solution)/shard_map/ppermute | solution.py:21
  0.8 25.0 %collective-permute-start.2 = (bf16[256,2048]{1,0:T(8,128)(2,1)}, bf16[256,2048]{1,0:T(8,128)(2,1)}, u32[]{:S(2)}, u32[]{:S(2)}) collective-permute-start(bf16[256,2048]{1,0:T(8,128)(2,1)} %param.17), channel_id=1, source_target_pairs={{0,2},{1,3},{2,0},{3,1},{4,6},{5,7},{6,4},{7,5},{8,10},{9,11},{10,... | collective-permute-start | bytes 3145736 | tf_op jit(solution)/shard_map/ppermute | solution.py:21
  3.0 5.5 %collective-permute-start = (bf16[2,128,64]{1,2,0:T(8,128)(2,1)S(1)}, bf16[2,128,64]{1,2,0:T(8,128)(2,1)S(1)}, u32[]{:S(2)}, u32[]{:S(2)}) collective-permute-start(bf16[2,128,64]{1,2,0:T(8,128)(2,1)S(1)} %pad_maximum_fusion), channel_id=1, source_target_pairs={{0,4},{4,8},{8,12},{1,5},{5,9},{9,13},{2,6},{6,10},{10,14},{3,7},{... | collective-permute-start | bytes 98312 | tf_op jit(solution)/shard_map/ppermute | solution.py:17
  8.3 0.7 copy-start.8
  9.5 18.9 %copy-start.2 = (bf16[256,2048]{1,0:T(8,128)(2,1)S(1)}, bf16[256,2048]{1,0:T(8,128)(2,1)}, u32[]{:S(2)}) copy-start(bf16[256,2048]{1,0:T(8,128)(2,1)} %param.17) | copy-start | bytes 3145732
  10.7 17.7 %all-to-all-start = ((bf16[4,128,256]{1,2,0:T(8,128)(2,1)}), bf16[4,128,256]{1,2,0:T(8,128)(2,1)S(1)}, u32[]{:S(2)}, u32[]{:S(2)}) async-start(bf16[4,128,256]{1,2,0:T(8,128)(2,1)} %bitcast.119), calls=%async_computation | async-start | bytes 524288 | tf_op jit(solution)/shard_map/all_to_all | solution.py:118
  25.7 6.3 %collective-permute-start.3 = (bf16[256,2048]{1,0:T(8,128)(2,1)}, bf16[256,2048]{1,0:T(8,128)(2,1)}, u32[]{:S(2)}, u32[]{:S(2)}) collective-permute-start(bf16[256,2048]{1,0:T(8,128)(2,1)} %collective-permute-done.2), channel_id=1, source_target_pairs={{0,1},{1,0},{2,3},{3,2},{4,5},{5,4},{6,7},{7,6},{8,9},{9,8},{10,11... | collective-permute-start | bytes 3145736 | tf_op jit(solution)/shard_map/ppermute | solution.py:21
  30.3 1.7 %copy-start.4 = (bf16[128,2048]{1,0:T(8,128)(2,1)S(1)}, bf16[128,2048]{1,0:T(8,128)(2,1)}, u32[]{:S(2)}) copy-start(bf16[128,2048]{1,0:T(8,128)(2,1)} %param.16) | copy-start | bytes 1572868
  32.0 1.8 %copy-start.3 = (bf16[128,2,512]{2,0,1:T(8,128)(2,1)S(1)}, bf16[128,2,512]{2,0,1:T(8,128)(2,1)}, u32[]{:S(2)}) copy-start(bf16[128,2,512]{2,0,1:T(8,128)(2,1)} %get-tuple-element.16) | copy-start | bytes 786436
  32.0 1.8 %copy-start.7 = (f32[2048]{0:T(1024)S(1)}, f32[2048]{0:T(1024)}, u32[]{:S(2)}) copy-start(f32[2048]{0:T(1024)} %param.18) | copy-start | bytes 24580
  34.6 55.3 %copy-start.10 = (bf16[1,2048,512]{2,1,0:T(8,128)(2,1)S(1)}, bf16[1,2048,512]{2,1,0:T(8,128)(2,1)}, u32[]{:S(2)}) copy-start(bf16[1,2048,512]{2,1,0:T(8,128)(2,1)} %param.19) | copy-start | bytes 6291460
  88.6 1.3 copy-start.1
  98.4 5.2 %copy-start.9 = (f32[128,2]{0,1:T(2,128)S(1)}, f32[128,2]{0,1:T(2,128)}, u32[]{:S(2)}) copy-start(f32[128,2]{0,1:T(2,128)} %param.23) | copy-start | bytes 3076
  98.4 52.7 %all-to-all-start.2 = ((bf16[16,32,2048]{2,1,0:T(8,128)(2,1)}), bf16[16,32,2048]{2,1,0:T(8,128)(2,1)}, u32[]{:S(2)}, u32[]{:S(2)}) async-start(bf16[16,32,2048]{2,1,0:T(8,128)(2,1)} %bitcast.111), calls=%async_computation.2 | async-start | bytes 4194304 | tf_op jit(solution)/shard_map/all_to_all | solution.py:152

commit v2 on v1

--- a/solution.py
+++ b/solution.py
@@ -5,6 +5,7 @@
 
 HDIM = 64
 WINDOW = 128
+GROUPS = 4
 
 
 rope_base = 10000.0
@@ -40,6 +41,11 @@
     before = jnp.dot(earlier, either, preferred_element_type=jnp.float32)
     rank = jnp.sum(before[:, None, :] * named.astype(jnp.float32), axis=-1).astype(jnp.int32)
     return routes * capacity + rank
+
+
+def turned_by(block, axis, distance):
+    count = lax.axis_size(axis)
+    return lax.ppermute(block, axis, [(i, (i + distance) % count) for i in range(count)])
 
 
 def rotate(rows, positions, heads):
@@ -55,6 +61,143 @@
         [lower * cosines - upper * sines, upper * cosines + lower * sines], axis=-1
     )
     return turned.reshape(rows.shape[0], heads * HDIM).astype(jnp.bfloat16)
+
+
+def plan_planes(routes, route_weight):
+    planes, lanes = lax.axis_size("sp"), lax.axis_size("tp")
+    plane, lane = lax.axis_index("sp"), lax.axis_index("tp")
+    count = routes.shape[0]
+    rows = lanes * (4 * count // (planes * lanes)) // 2
+    capacity = 4 * count // (planes * lanes)
+    meta = jnp.concatenate([routes.astype(jnp.float32), route_weight], axis=1).T
+    metas = jnp.stack([meta] + [turned_by(meta, "sp", d) for d in range(1, planes)])
+    row = jnp.arange(count, dtype=jnp.int32)
+    earlier = (row[:, None] < row[None, :]).astype(jnp.bfloat16)
+
+    def ranked(named):
+        return jnp.einsum(
+            "...tm,mn->...tn", named.astype(jnp.bfloat16), earlier, preferred_element_type=jnp.float32
+        )
+
+    own = routes[:, 0] // lanes
+    in_plane = jnp.arange(planes, dtype=jnp.int32)[:, None] == own[None, :]
+    own_rank = jnp.sum(jnp.where(in_plane, ranked(in_plane), 0.0), axis=0).astype(jnp.int32)
+    key = lax.rem(own - plane + planes, planes) * rows + own_rank
+    send = (jnp.arange(planes * rows, dtype=jnp.int32)[:, None] == key[None, :]).astype(jnp.bfloat16)
+
+    experts = metas[:, :2].astype(jnp.int32)
+    mine = experts[:, 0] // lanes == plane
+    local = lax.rem(experts, lanes)
+    named = (local[:, :, None, :] == jnp.arange(lanes, dtype=jnp.int32)[:, None]) & mine[:, None, None]
+    before = ranked(named[:, 0] | named[:, 1])
+    rank = jnp.sum(jnp.where(named, before[:, None], 0.0), axis=2).astype(jnp.int32)
+    slot = jnp.where(mine[:, None], (local ^ lane) * capacity + rank, -1)
+    spot = slot[:, :, None, :] == jnp.arange(lanes * capacity, dtype=jnp.int32)[:, None]
+    mine_rank = ranked(mine[:, None])[:, 0].astype(jnp.int32)
+    line = (mine_rank[:, None] == jnp.arange(rows, dtype=jnp.int32)[:, None]) & mine[:, None]
+    spread = jnp.einsum(
+        "dsn,drn->dsr",
+        (spot[:, 0] | spot[:, 1]).astype(jnp.bfloat16),
+        line.astype(jnp.bfloat16),
+        preferred_element_type=jnp.float32,
+    ).astype(jnp.bfloat16)
+    weighted = jnp.sum(jnp.where(spot, metas[:, 2:, None], 0.0), axis=1)
+    fold = jnp.einsum(
+        "drn,dsn->drs",
+        line.astype(jnp.float32),
+        weighted,
+        precision=lax.Precision.HIGHEST,
+        preferred_element_type=jnp.float32,
+    )
+    coarse = fold.astype(jnp.bfloat16)
+    fine = (fold - coarse.astype(jnp.float32)).astype(jnp.bfloat16)
+    return send, spread, coarse, fine
+
+
+def lane_exchange(blocks):
+    offset = lax.axis_size("tp") // 2
+    while offset:
+        keep = [m for m in sorted(blocks) if not m & offset]
+        go = [m for m in sorted(blocks) if m & offset]
+        size = blocks[0].shape[0]
+        came = swapped(jnp.concatenate([blocks[m] for m in go]), "tp", offset)
+        for i, m in enumerate(go):
+            blocks[m] = came[i * size : (i + 1) * size]
+        offset //= 2
+    return blocks
+
+
+def plane_experts(stream_f, normed, plans, gate, up, down):
+    send, spread, coarse, fine = plans
+    planes, lanes = lax.axis_size("sp"), lax.axis_size("tp")
+    rows = send.shape[0] // planes
+    capacity = spread.shape[1] // lanes
+    leaving = jnp.dot(send, normed, preferred_element_type=jnp.float32).astype(jnp.bfloat16)
+    came = [leaving[:rows]]
+    for d in range(1, planes):
+        came.append(turned_by(leaving[d * rows : (d + 1) * rows], "sp", d))
+
+    def lanes_apart(block):
+        return {m: block[m * capacity : (m + 1) * capacity] for m in range(lanes)}
+
+    def joined(blocks):
+        return jnp.concatenate([blocks[m] for m in range(lanes)])
+
+    back = []
+    for d in range(planes):
+        slots = jnp.dot(spread[d], came[d], preferred_element_type=jnp.float32)
+        served = joined(lane_exchange(lanes_apart(slots.astype(jnp.bfloat16))))
+        gate_out = jnp.dot(served, gate, preferred_element_type=jnp.float32)
+        up_out = jnp.dot(served, up, preferred_element_type=jnp.float32)
+        hidden = (jax.nn.silu(gate_out) * up_out).astype(jnp.bfloat16)
+        produced = jnp.dot(hidden, down, preferred_element_type=jnp.float32).astype(jnp.bfloat16)
+        returned = joined(lane_exchange(lanes_apart(produced)))
+        folded = jnp.dot(coarse[d], returned, preferred_element_type=jnp.float32)
+        folded = folded + jnp.dot(fine[d], returned, preferred_element_type=jnp.float32)
+        folded = folded.astype(jnp.bfloat16)
+        back.append(turned_by(folded, "sp", planes - d) if d else folded)
+    total = stream_f
+    for d in range(planes):
+        total = total + jnp.einsum(
+            "rn,rd->nd",
+            send[d * rows : (d + 1) * rows],
+            back[d],
+            preferred_element_type=jnp.float32,
+        )
+    return total.astype(jnp.bfloat16)
+
+
+def direct_experts(stream_f, normed, plans, gate, up, down, routes, route_weight):
+    row_count = normed.shape[0]
+    sp_count = lax.axis_size("sp")
+    tp_count = lax.axis_size("tp")
+    expert_count = sp_count * tp_count
+    capacity = 4 * row_count // expert_count
+    width = normed.shape[1]
+    slot_index = slots_of(routes, expert_count, capacity)
+    slot_ids = jnp.arange(expert_count * capacity, dtype=jnp.int32)
+    place = (slot_index[:, :, None] == slot_ids[None, None, :]).astype(jnp.bfloat16)
+    outgoing = jnp.einsum(
+        "ns,nd->sd", place[:, 0] + place[:, 1], normed, preferred_element_type=jnp.float32
+    ).astype(jnp.bfloat16)
+    outgoing = outgoing.reshape(expert_count, capacity, width)
+    arrived = lax.all_to_all(outgoing, ("sp", "tp"), split_axis=0, concat_axis=0, tiled=True)
+    flat_rows = arrived.reshape(-1, width)
+    gate_out = jnp.dot(flat_rows, gate, preferred_element_type=jnp.float32)
+    up_out = jnp.dot(flat_rows, up, preferred_element_type=jnp.float32)
+    hidden = (jax.nn.silu(gate_out) * up_out).astype(jnp.bfloat16)
+    produced = jnp.dot(hidden, down, preferred_element_type=jnp.float32).astype(
+        jnp.bfloat16
+    )
+    returned = lax.all_to_all(
+        produced.reshape(arrived.shape), ("sp", "tp"), split_axis=0, concat_axis=0, tiled=True
+    )
+    returned = returned.reshape(expert_count * capacity, width)
+    total = stream_f
+    for k in range(2):
+        picked = jnp.dot(place[:, k], returned, preferred_element_type=jnp.float32)
+        total = total + picked * route_weight[:, k : k + 1]
+    return total.astype(jnp.bfloat16)
 
 
 def per_device(
@@ -71,6 +214,7 @@
     routes,
     route_weight,
 ):
+    plans = plan_planes(routes, route_weight) if lax.axis_size("sp") == GROUPS else None
     weight_of = gathered_by_doubling(out_weight, "tp")
     tok_count = query_rows.shape[0]
     head_local = query_rows.shape[1] // HDIM
@@ -129,35 +273,10 @@
         * lax.rsqrt(jnp.mean(stream_f * stream_f, axis=-1, keepdims=True) + norm_eps)
         * norm_gain[None, :]
     ).astype(jnp.bfloat16)
-    sp_count = lax.axis_size("sp")
-    tp_count = lax.axis_size("tp")
-    expert_count = sp_count * tp_count
-    capacity = 4 * row_count // expert_count
-    width = normed.shape[1]
-    slot_index = slots_of(routes, expert_count, capacity)
-    slot_ids = jnp.arange(expert_count * capacity, dtype=jnp.int32)
-    place = (slot_index[:, :, None] == slot_ids[None, None, :]).astype(jnp.bfloat16)
-    outgoing = jnp.einsum(
-        "ns,nd->sd", place[:, 0] + place[:, 1], normed, preferred_element_type=jnp.float32
-    ).astype(jnp.bfloat16)
-    outgoing = outgoing.reshape(expert_count, capacity, width)
-    arrived = lax.all_to_all(outgoing, ("sp", "tp"), split_axis=0, concat_axis=0, tiled=True)
-    flat_rows = arrived.reshape(-1, width)
-    gate_out = jnp.dot(flat_rows, gate_weight[0], preferred_element_type=jnp.float32)
-    up_out = jnp.dot(flat_rows, up_weight[0], preferred_element_type=jnp.float32)
-    hidden = (jax.nn.silu(gate_out) * up_out).astype(jnp.bfloat16)
-    produced = jnp.dot(hidden, down_weight[0], preferred_element_type=jnp.float32).astype(
-        jnp.bfloat16
-    )
-    returned = lax.all_to_all(
-        produced.reshape(arrived.shape), ("sp", "tp"), split_axis=0, concat_axis=0, tiled=True
-    )
-    returned = returned.reshape(expert_count * capacity, width)
-    total = stream_f
-    for k in range(2):
-        picked = jnp.dot(place[:, k], returned, preferred_element_type=jnp.float32)
-        total = total + picked * route_weight[:, k : k + 1]
-    return total.astype(jnp.bfloat16)
+    args = (stream_f, normed, plans, gate_weight[0], up_weight[0], down_weight[0])
+    if lax.axis_size("sp") == GROUPS:
+        return plane_experts(*args)
+    return direct_experts(*args, routes, route_weight)
 
 
 def solution(mesh):

time: 157 us -> 159 us (1.013); the launches traced: 156 us -> 156 us
  blocking collectives: 54 us -> 0 us
  local copies, waits for them, and re-layouts: 3.28 us -> 36.1 us
  waiting for transfers between devices: 57.8 us -> 33.6 us
  starting transfers between devices: 15.9 us -> 35.1 us
  matrix products: 21.3 us -> 39.8 us
  other arithmetic: 3.37 us -> 10.5 us
    all_to_all x1 -> x0, blocking collectives: 54 us -> none  [per_device(): lax.all_to_all(outgoing, ('sp', 'tp'), split_axis=0, concat_axis=0, tiled...]
    all_to_all x1 -> x0, waiting for transfers between devices: 47.5 us -> none  [per_device(): lax.all_to_all(produced.reshape(arrived.shape), ('sp', 'tp'), split_axis=...]
    ppermute x0 -> x9, waiting for transfers between devices: none -> 29.7 us  [turned_by(): lax.ppermute(block, axis, [(i, (i + distance) % count) for i in range(cou...]
    slice x0 -> x25, local copies, waits for them, and re-layouts: none -> 22.9 us  [the longest x16 15.9 us: lane_exchange(): blocks[m] = came[i * size:(i + 1) * size]]
    dot_general x6 -> x29, matrix products: 14.4 us -> 32.8 us  [the longest x4 14 us: plane_experts(): jnp.dot(hidden, down, preferred_element_type=jnp.float32)]
    ppermute x3 -> x19, starting transfers between devices: 2.47 us -> 16 us  [swapped(): lax.ppermute(block, axis, [(i, i ^ offset) for i in range(lax.axis_size(a...]
    ppermute x0 -> x9, starting transfers between devices: none -> 10.7 us  [turned_by(): lax.ppermute(block, axis, [(i, (i + distance) % count) for i in range(cou...]
    ppermute x3 -> x19, waiting for transfers between devices: 9.88 us -> 0.38 us  [swapped(): lax.ppermute(block, axis, [(i, i ^ offset) for i in range(lax.axis_size(a...]
  transfers between devices with their start and end apart: 6 -> 30, of which waited for: 3 -> 8; matrix products, arithmetic and copies ran while one was open for 7% -> 51% of each run, Pallas kernels for 0% -> 0%
where the time goes in v2:
time: 159 us; the launch traced here: 156 us
  matrix products  39.8 us (25%)
  local copies, waits for them, and re-layouts  36.1 us (23%)
  starting transfers between devices  35.1 us (22%)
  waiting for transfers between devices  33.6 us (21%)
  other arithmetic  10.5 us (7%)
    ppermute x9, waiting for transfers between devices, turned_by(): lax.ppermute(block, axis, [(i, (i + distance) % count) for i in range(cou...  29.7 us
    ppermute x19, starting transfers between devices, swapped(): lax.ppermute(block, axis, [(i, i ^ offset) for i in range(lax.axis_size(a...  16 us
    slice x16, local copies, waits for them, and re-layouts, lane_exchange(): blocks[m] = came[i * size:(i + 1) * size]  15.9 us
    dot_general x4, matrix products, plane_experts(): jnp.dot(hidden, down, preferred_element_type=jnp.float32)  14 us
    ppermute x9, starting transfers between devices, turned_by(): lax.ppermute(block, axis, [(i, (i + distance) % count) for i in range(cou...  10.7 us
    concatenate x8, local copies, waits for them, and re-layouts, lane_exchange(): came = swapped(jnp.concatenate([blocks[m] for m in go]), 'tp', offset)  7.77 us
    slice x8, local copies, waits for them, and re-layouts, lanes_apart(): return {m: block[m * capacity:(m + 1) * capacity] for m in range(lanes)}  6.95 us
    all_to_all x1, starting transfers between devices, per_device(): lax.all_to_all(attended, 'tp', split_axis=0, concat_axis=1, tiled=True)  6.43 us
  transfers between devices with their start and end apart: 30, of which 8 were waited for; matrix products, arithmetic and copies ran while one was open for 51% of the time, Pallas kernels for 0%

profile of v2, /device:TPU:11, one launch (start us, length us, event | category | flops | bytes accessed | tf_op | source)
XLA Modules:
  0.0 155.9 jit_solution(10290060682655976696)
XLA Ops:
  0.0 0.7 collective-permute-start.1
  2.4 1.3 collective-permute-start.4
  3.7 1.1 collective-permute-start.5
  4.8 1.4 collective-permute-start.6
  6.2 0.9 bitcast_convert_fusion
  9.2 1.1 copy.34
  11.7 2.0 %collective-permute-start = (bf16[2,128,64]{1,2,0:T(8,128)(2,1)S(1)}, bf16[2,128,64]{1,2,0:T(8,128)(2,1)S(1)}, u32[]{:S(2)}, u32[]{:S(2)}) collective-permute-start(bf16[2,128,64]{1,2,0:T(8,128)(2,1)S(1)} %pad_maximum_fusion.37), channel_id=1, source_target_pairs={{0,4},{4,8},{8,12},{1,5},{5,9},{9,13},{2,6},{6,10},{10,14},{3,7},{... | collective-permute-start | bytes 98312 | tf_op jit(solution)/shard_map/ppermute | solution.py:18
  14.2 1.0 subtract_convert_fusion.1
  15.3 1.5 collective-permute-done
  17.8 1.2 convolution_convert_fusion.9
  19.0 6.4 %all-to-all-start = ((bf16[4,128,256]{1,2,0:T(8,128)(2,1)}), bf16[4,128,256]{1,2,0:T(8,128)(2,1)S(1)}, u32[]{:S(2)}, u32[]{:S(2)}) async-start(bf16[4,128,256]{1,2,0:T(8,128)(2,1)} %bitcast.214), calls=%async_computation | async-start | bytes 524288 | tf_op jit(solution)/shard_map/all_to_all | solution.py:262
  25.7 0.9 collective-permute-start.3
  26.7 0.8 convolution_convert_fusion.10
  27.5 2.1 %all-to-all-done = bf16[4,128,256]{1,2,0:T(8,128)(2,1)S(1)} async-done(((bf16[4,128,256]{1,2,0:T(8,128)(2,1)}), bf16[4,128,256]{1,2,0:T(8,128)(2,1)S(1)}, u32[]{:S(2)}, u32[]{:S(2)}) %all-to-all-start) | async-done | bytes 262176 | tf_op jit(solution)/shard_map/all_to_all | solution.py:262
  29.9 1.6 %convolution_add_fusion.4 = f32[128,2048]{1,0:T(8,128)S(1)} fusion(f32[128,2048]{1,0:T(8,128)S(1)} %fusion.92, bf16[256,2048]{1,0:T(8,128)(2,1)} %collective-permute-done.1, bf16[128,1024]{0,1:T(8,128)(2,1)S(1)} %bitcast.210, s32[]{:T(128)S(6)} %select_n.58), kind=kOutput, calls=%fused_computation.8 | convolution fusion | flops 134479872 | bytes 3211268 | tf_op jit(solution)/shard_map/dot_general | solution.py:267
  31.5 1.6 %convolution_add_fusion.3 = f32[128,2048]{1,0:T(8,128)S(1)} fusion(f32[128,2048]{1,0:T(8,128)S(1)} %convolution_add_fusion.4, bf16[256,2048]{1,0:T(8,128)(2,1)} %collective-permute-done.2, bf16[128,1024]{0,1:T(8,128)(2,1)S(1)} %bitcast.211, s32[]{:T(128)S(6)} %select_n.59), kind=kOutput, calls=%fused_computation.7 | convolution fusion | flops 134479872 | bytes 3211268 | tf_op jit(solution)/shard_map/dot_general | solution.py:267
  33.2 1.7 %multiply_reduce_fusion = (f32[128]{0:T(128)S(1)}, f32[128,2048]{1,0:T(8,128)S(1)}) fusion(f32[128,2048]{1,0:T(8,128)S(1)} %convolution_add_fusion.3, bf16[256,2048]{1,0:T(8,128)(2,1)} %collective-permute-done.3, bf16[128,1024]{0,1:T(8,128)(2,1)S(1)} %bitcast.212, s32[]{:T(128)S(6)} %select_n.60, bf16[128,2048]{1,0:T(8,128)(2,1)S(1)} %copy-done.5), kind=kOutput, calls=%fused_computation.59 | convolution fusion | flops 136052608 | bytes 3736068 | tf_op jit(solution)/shard_map/dot_general | solution.py:267
  36.1 1.0 collective-permute-start.7
  37.1 1.4 collective-permute-start.17
  39.1 3.7 %collective-permute-done.11 = bf16[64,2048]{1,0:T(8,128)(2,1)S(1)} collective-permute-done((bf16[64,2048]{1,0:T(8,128)(2,1)S(1)}, bf16[64,2048]{1,0:T(8,128)(2,1)S(1)}, u32[]{:S(2)}, u32[]{:S(2)}) %collective-permute-start.11) | collective-permute-done | bytes 262176 | tf_op jit(solution)/shard_map/ppermute | solution.py:48
  43.9 3.6 %collective-permute-start.8 = (bf16[64,2048]{1,0:T(8,128)(2,1)S(1)}, bf16[64,2048]{1,0:T(8,128)(2,1)S(1)}, u32[]{:S(2)}, u32[]{:S(2)}) collective-permute-start(bf16[64,2048]{1,0:T(8,128)(2,1)S(1)} %pad_maximum_fusion.8), channel_id=1, source_target_pairs={{0,1},{1,0},{2,3},{3,2},{4,5},{5,4},{6,7},{7,6},{8,9},{9,8},{10,11... | collective-permute-start | bytes 786440 | tf_op jit(solution)/shard_map/ppermute | solution.py:22
  48.1 9.1 %collective-permute-done.17 = bf16[64,2048]{1,0:T(8,128)(2,1)S(1)} collective-permute-done((bf16[64,2048]{1,0:T(8,128)(2,1)S(1)}, bf16[64,2048]{1,0:T(8,128)(2,1)S(1)}, u32[]{:S(2)}, u32[]{:S(2)}) %collective-permute-start.17) | collective-permute-done | bytes 262176 | tf_op jit(solution)/shard_map/ppermute | solution.py:48
  58.3 0.9 collective-permute-start.18
  59.8 0.9 collective-permute-done.23
  61.8 1.0 collective-permute-start.24
  64.8 1.1 collective-permute-start.13
  66.6 1.1 fusion.20
  67.8 3.4 %convolution_convert_fusion.7 = bf16[128,2048]{1,0:T(8,128)(2,1)} fusion(bf16[1,512,2048]{2,1,0:T(8,128)(2,1)S(1)} %copy-done, f32[128,512]{1,0:T(8,128)} %fusion.20, bf16[1,2048,512]{2,1,0:T(8,128)(2,1)} %param.19, bf16[32,2048]{1,0:T(8,128)(2,1)} %copy-done.22, bf16[32,2048]{1,0:T(8,128)(2,1)} %copy-done.18, bf16[32,2048]{1,0:T(8,128)(2,1)} %copy-done.21, ...), kind=kOutput, calls=%fused_computation.18 | convolution fusion | flops 539623424 | bytes 5505024 | tf_op jit(solution)/shard_map/dot_general | solution.py:153
  71.2 1.8 %concatenate.126 = bf16[64,2048]{1,0:T(8,128)(2,1)} slice(bf16[128,2048]{1,0:T(8,128)(2,1)} %convolution_convert_fusion.7), slice={[64:128], [0:2048]} | slice | bytes 524288 | tf_op jit(solution)/shard_map/concatenate | solution.py:123
  73.1 0.8 collective-permute-start.9
  73.9 1.6 %fusion.173 = (bf16[32,2048]{1,0:T(8,128)(2,1)}, bf16[32,2048]{1,0:T(8,128)(2,1)S(1)}) fusion(bf16[64,2048]{1,0:T(8,128)(2,1)} %collective-permute-done.18), kind=kLoop, calls=%fused_computation.270 | loop fusion | bytes 524288 | tf_op jit(solution)/shard_map/slice | solution.py:125
  76.6 1.6 %fusion.177 = (bf16[32,2048]{1,0:T(8,128)(2,1)}, bf16[32,2048]{1,0:T(8,128)(2,1)S(1)}) fusion(bf16[64,2048]{1,0:T(8,128)(2,1)} %collective-permute-done.24), kind=kLoop, calls=%fused_computation.274 | loop fusion | bytes 524288 | tf_op jit(solution)/shard_map/slice | solution.py:125
  79.2 1.0 fusion.164
  80.9 1.2 fusion.18
  82.1 3.4 %convolution_convert_fusion.5 = bf16[128,2048]{1,0:T(8,128)(2,1)} fusion(bf16[1,512,2048]{2,1,0:T(8,128)(2,1)S(1)} %copy-done, f32[128,512]{1,0:T(8,128)} %fusion.18, bf16[1,2048,512]{2,1,0:T(8,128)(2,1)} %param.19, bf16[32,2048]{1,0:T(8,128)(2,1)} %copy-done.24, bf16[32,2048]{1,0:T(8,128)(2,1)} %get-tuple-element.34, bf16[32,2048]{1,0:T(8,128)(2,1)} %copy-done.23, ...), kind=kOutput, calls=%fused_computation.16 | convolution fusion | flops 539623424 | bytes 5505024 | tf_op jit(solution)/shard_map/dot_general | solution.py:153
  85.5 1.8 %concatenate.128 = bf16[64,2048]{1,0:T(8,128)(2,1)} slice(bf16[128,2048]{1,0:T(8,128)(2,1)} %convolution_convert_fusion.5), slice={[64:128], [0:2048]} | slice | bytes 524288 | tf_op jit(solution)/shard_map/concatenate | solution.py:123
  88.0 1.0 fusion.167
  90.3 1.6 %fusion.154 = (bf16[32,2048]{1,0:T(8,128)(2,1)}, bf16[32,2048]{1,0:T(8,128)(2,1)S(1)}) fusion(bf16[128,2048]{1,0:T(8,128)(2,1)} %convolution_convert_fusion.5), kind=kLoop, calls=%fused_computation.251 | loop fusion | bytes 524288 | tf_op jit(solution)/shard_map/slice | solution.py:141
  91.9 1.0 fusion.172
  93.6 1.2 fusion.16
  94.8 3.6 %convolution_convert_fusion.3 = bf16[128,2048]{1,0:T(8,128)(2,1)} fusion(bf16[1,512,2048]{2,1,0:T(8,128)(2,1)S(1)} %copy-done, f32[128,512]{1,0:T(8,128)} %fusion.16, bf16[1,2048,512]{2,1,0:T(8,128)(2,1)} %param.19, bf16[32,2048]{1,0:T(8,128)(2,1)} %copy-done.26, bf16[32,2048]{1,0:T(8,128)(2,1)} %get-tuple-element.50, bf16[32,2048]{1,0:T(8,128)(2,1)} %copy-done.25, ...), kind=kOutput, calls=%fused_computation.14 | convolution fusion | flops 539623424 | bytes 5505024 | tf_op jit(solution)/shard_map/dot_general | solution.py:153
  98.3 1.7 %concatenate.130 = bf16[64,2048]{1,0:T(8,128)(2,1)} slice(bf16[128,2048]{1,0:T(8,128)(2,1)} %convolution_convert_fusion.3), slice={[64:128], [0:2048]} | slice | bytes 524288 | tf_op jit(solution)/shard_map/concatenate | solution.py:123
  100.0 0.9 collective-permute-start.20
  100.9 1.7 %fusion.158 = (bf16[32,2048]{1,0:T(8,128)(2,1)}, bf16[32,2048]{1,0:T(8,128)(2,1)}) fusion(bf16[128,2048]{1,0:T(8,128)(2,1)} %convolution_convert_fusion.3), kind=kLoop, calls=%fused_computation.255 | loop fusion | bytes 524288 | tf_op jit(solution)/shard_map/slice | solution.py:141
  102.5 1.0 fusion.176
  104.2 2.9 %fusion.14 = f32[128,512]{1,0:T(8,128)} fusion(bf16[1,2048,512]{2,1,0:T(8,128)(2,1)} %param.20, bf16[32,2048]{1,0:T(8,128)(2,1)S(1)} %get-tuple-element.57, bf16[32,2048]{1,0:T(8,128)(2,1)} %get-tuple-element.58, bf16[32,2048]{1,0:T(8,128)(2,1)S(1)} %get-tuple-element.56, bf16[32,2048]{1,0:T(8,128)(2,1)} %get-tuple-element.26), kind=kOutput, calls=%fused_computation.33 | convolution fusion | flops 270532608 | bytes 2883584 | tf_op jit(solution)/shard_map/dot_general | solution.py:151
  107.1 3.6 %convolution_convert_fusion.1 = bf16[128,2048]{1,0:T(8,128)(2,1)} fusion(bf16[1,512,2048]{2,1,0:T(8,128)(2,1)S(1)} %copy-done, f32[128,512]{1,0:T(8,128)} %fusion.14, bf16[1,2048,512]{2,1,0:T(8,128)(2,1)} %param.19, bf16[32,2048]{1,0:T(8,128)(2,1)} %copy-done.28, bf16[32,2048]{1,0:T(8,128)(2,1)} %get-tuple-element.58, bf16[32,2048]{1,0:T(8,128)(2,1)} %copy-done.27, ...), kind=kOutput, calls=%fused_computation.12 | convolution fusion | flops 539623424 | bytes 5505024 | tf_op jit(solution)/shard_map/dot_general | solution.py:153
  110.7 1.0 concatenate.132
  112.4 1.6 %fusion.160 = (bf16[32,2048]{1,0:T(8,128)(2,1)}, bf16[32,2048]{1,0:T(8,128)(2,1)S(1)}) fusion(bf16[128,2048]{1,0:T(8,128)(2,1)} %convolution_convert_fusion.1), kind=kLoop, calls=%fused_computation.257 | loop fusion | bytes 524288 | tf_op jit(solution)/shard_map/slice | solution.py:141
  114.0 1.6 %fusion.163 = (bf16[32,2048]{1,0:T(8,128)(2,1)}, bf16[32,2048]{1,0:T(8,128)(2,1)S(1)}) fusion(bf16[64,2048]{1,0:T(8,128)(2,1)} %collective-permute-done.14), kind=kLoop, calls=%fused_computation.260 | loop fusion | bytes 524288 | tf_op jit(solution)/shard_map/slice | solution.py:125
  116.9 1.6 %fusion.171 = (bf16[32,2048]{1,0:T(8,128)(2,1)}, bf16[32,2048]{1,0:T(8,128)(2,1)S(1)}) fusion(bf16[64,2048]{1,0:T(8,128)(2,1)} %collective-permute-done.20), kind=kLoop, calls=%fused_computation.268 | loop fusion | bytes 524288 | tf_op jit(solution)/shard_map/slice | solution.py:125
  120.7 1.2 collective-permute-start.27
  121.9 1.0 fusion.166
  123.5 1.7 %fusion.83 = f32[64,2048]{1,0:T(8,128)} fusion(bf16[32,2048]{1,0:T(8,128)(2,1)S(1)} %get-tuple-element.37, bf16[32,2048]{1,0:T(8,128)(2,1)S(1)} %get-tuple-element.38, bf16[32,2048]{1,0:T(8,128)(2,1)S(1)} %get-tuple-element.36, bf16[32,2048]{1,0:T(8,128)(2,1)S(1)} %get-tuple-element.16, bf16[4,64,128]{2,1,0:T(8,128)(2,1)} %get-tuple-element.5), kind=kOutput, calls=%fused_computation.129 | convolution fusion | flops 35651584 | bytes 1064960 | tf_op jit(solution)/shard_map/dot_general | solution.py:156
  125.3 2.5 %convolution_add_fusion.1 = f32[128,2048]{1,0:T(8,128)} fusion(f32[128,2048]{1,0:T(8,128)S(1)} %get-tuple-element.73, f32[64,2048]{1,0:T(8,128)} %fusion.83, bf16[32,2048]{1,0:T(8,128)(2,1)} %copy-done.4, bf16[32,2048]{1,0:T(8,128)(2,1)S(1)} %get-tuple-element.38, bf16[32,2048]{1,0:T(8,128)(2,1)S(1)} %get-tuple-element.36, ...), kind=kOutput, calls=%fused_computation.4 | convolution fusion | flops 69730304 | bytes 3170304 | tf_op jit(solution)/shard_map/rn,rd->nd/dot_general | solution.py:161
  127.8 1.0 fusion.170
  128.9 1.2 fusion.81
  130.4 3.2 %collective-permute-start.22 = (bf16[64,2048]{1,0:T(8,128)(2,1)S(1)}, bf16[64,2048]{1,0:T(8,128)(2,1)S(1)}, u32[]{:S(2)}, u32[]{:S(2)}) collective-permute-start(bf16[64,2048]{1,0:T(8,128)(2,1)S(1)} %fusion.8), channel_id=1, source_target_pairs={{0,8},{4,12},{8,0},{12,4},{1,9},{5,13},{9,1},{13,5},{2,10},{6,14},... | collective-permute-start | bytes 786440 | tf_op jit(solution)/shard_map/ppermute | solution.py:48
  133.5 1.0 fusion.174
  135.1 1.0 fusion.162
  136.6 1.5 collective-permute-start.16
  138.1 5.0 %collective-permute-done.22 = bf16[64,2048]{1,0:T(8,128)(2,1)S(1)} collective-permute-done((bf16[64,2048]{1,0:T(8,128)(2,1)S(1)}, bf16[64,2048]{1,0:T(8,128)(2,1)S(1)}, u32[]{:S(2)}, u32[]{:S(2)}) %collective-permute-start.22) | collective-permute-done | bytes 262176 | tf_op jit(solution)/shard_map/ppermute | solution.py:48
  143.4 11.0 %collective-permute-done.28 = bf16[64,2048]{1,0:T(8,128)(2,1)S(1)} collective-permute-done((bf16[64,2048]{1,0:T(8,128)(2,1)S(1)}, bf16[64,2048]{1,0:T(8,128)(2,1)S(1)}, u32[]{:S(2)}, u32[]{:S(2)}) %collective-permute-start.28) | collective-permute-done | bytes 262176 | tf_op jit(solution)/shard_map/ppermute | solution.py:48
  154.8 1.2 fusion.5
  (193 shorter events, 28.8 us)
Async XLA Ops:
  0.0 67.8 %copy-start = (bf16[1,512,2048]{2,1,0:T(8,128)(2,1)S(1)}, bf16[1,512,2048]{2,1,0:T(8,128)(2,1)}, u32[]{:S(2)}) copy-start(bf16[1,512,2048]{2,1,0:T(8,128)(2,1)} %param.21) | copy-start | bytes 6291460
  0.0 10.6 %copy-start.33 = (s32[128,2]{0,1:T(2,128)S(1)}, s32[128,2]{0,1:T(2,128)}, u32[]{:S(2)}) copy-start(s32[128,2]{0,1:T(2,128)} %param.22) | copy-start | bytes 3076
  0.0 11.6 %copy-start.7 = (bf16[512,64]{0,1:T(8,128)(2,1)S(1)}, bf16[512,64]{0,1:T(8,128)(2,1)}, u32[]{:S(2)}) copy-start(bf16[512,64]{0,1:T(8,128)(2,1)} %param.14) | copy-start | bytes 196612
  0.0 11.6 %slice-start = ((bf16[512,64]{0,1:T(8,128)(2,1)}), bf16[384,64]{0,1:T(8,128)(2,1)S(1)}, s32[]{:S(2)}) async-start(bf16[512,64]{0,1:T(8,128)(2,1)} %param.14), calls=%async_computation.1 | async-start | bytes 98304 | tf_op jit(solution)/shard_map/slice | solution.py:237
  0.0 29.9 %collective-permute-start.1 = (bf16[256,2048]{1,0:T(8,128)(2,1)}, bf16[256,2048]{1,0:T(8,128)(2,1)}, u32[]{:S(2)}, u32[]{:S(2)}) collective-permute-start(bf16[256,2048]{1,0:T(8,128)(2,1)} %param.17), channel_id=1, source_target_pairs={{0,1},{1,0},{2,3},{3,2},{4,5},{5,4},{6,7},{7,6},{8,9},{9,8},{10,11... | collective-permute-start | bytes 3145736 | tf_op jit(solution)/shard_map/ppermute | solution.py:22
  0.8 25.0 %collective-permute-start.2 = (bf16[256,2048]{1,0:T(8,128)(2,1)}, bf16[256,2048]{1,0:T(8,128)(2,1)}, u32[]{:S(2)}, u32[]{:S(2)}) collective-permute-start(bf16[256,2048]{1,0:T(8,128)(2,1)} %param.17), channel_id=1, source_target_pairs={{0,2},{1,3},{2,0},{3,1},{4,6},{5,7},{6,4},{7,5},{8,10},{9,11},{10,... | collective-permute-start | bytes 3145736 | tf_op jit(solution)/shard_map/ppermute | solution.py:22
  2.4 9.3 %collective-permute-start.4 = (f32[4,128]{1,0:T(4,128)S(1)}, f32[4,128]{1,0:T(4,128)S(1)}, u32[]{:S(2)}, u32[]{:S(2)}) collective-permute-start(f32[4,128]{1,0:T(4,128)S(1)} %get-tuple-element.69), channel_id=1, source_target_pairs={{0,4},{4,8},{8,12},{12,0},{1,5},{5,9},{9,13},{13,1},{2,6},{6,10},{... | collective-permute-start | bytes 6152 | tf_op jit(solution)/shard_map/ppermute | solution.py:48
  3.7 10.0 %collective-permute-start.5 = (f32[4,128]{1,0:T(4,128)S(1)}, f32[4,128]{1,0:T(4,128)S(1)}, u32[]{:S(2)}, u32[]{:S(2)}) collective-permute-start(f32[4,128]{1,0:T(4,128)S(1)} %get-tuple-element.69), channel_id=1, source_target_pairs={{0,8},{4,12},{8,0},{12,4},{1,9},{5,13},{9,1},{13,5},{2,10},{6,14},... | collective-permute-start | bytes 6152 | tf_op jit(solution)/shard_map/ppermute | solution.py:48
  4.8 9.0 %collective-permute-start.6 = (f32[4,128]{1,0:T(4,128)S(1)}, f32[4,128]{1,0:T(4,128)S(1)}, u32[]{:S(2)}, u32[]{:S(2)}) collective-permute-start(f32[4,128]{1,0:T(4,128)S(1)} %get-tuple-element.69), channel_id=1, source_target_pairs={{0,12},{4,0},{8,4},{12,8},{1,13},{5,1},{9,5},{13,9},{2,14},{6,2},{... | collective-permute-start | bytes 6152 | tf_op jit(solution)/shard_map/ppermute | solution.py:48
  11.7 5.6 %copy-start.34 = (f32[4]{0:T(128)S(1)}, f32[4]{0:T(128)}, u32[]{:S(2)}) copy-start(f32[4]{0:T(128)} %param.15) | copy-start | bytes 52
  11.7 5.1 %collective-permute-start = (bf16[2,128,64]{1,2,0:T(8,128)(2,1)S(1)}, bf16[2,128,64]{1,2,0:T(8,128)(2,1)S(1)}, u32[]{:S(2)}, u32[]{:S(2)}) collective-permute-start(bf16[2,128,64]{1,2,0:T(8,128)(2,1)S(1)} %pad_maximum_fusion.37), channel_id=1, source_target_pairs={{0,4},{4,8},{8,12},{1,5},{5,9},{9,13},{2,6},{6,10},{10,14},{3,7},{... | collective-permute-start | bytes 98312 | tf_op jit(solution)/shard_map/ppermute | solution.py:18
  17.8 11.8 %copy-start.2 = (bf16[256,2048]{1,0:T(8,128)(2,1)S(1)}, bf16[256,2048]{1,0:T(8,128)(2,1)}, u32[]{:S(2)}) copy-start(bf16[256,2048]{1,0:T(8,128)(2,1)} %param.17) | copy-start | bytes 3145732
  19.0 10.6 %all-to-all-start = ((bf16[4,128,256]{1,2,0:T(8,128)(2,1)}), bf16[4,128,256]{1,2,0:T(8,128)(2,1)S(1)}, u32[]{:S(2)}, u32[]{:S(2)}) async-start(bf16[4,128,256]{1,2,0:T(8,128)(2,1)} %bitcast.214), calls=%async_computation | async-start | bytes 524288 | tf_op jit(solution)/shard_map/all_to_all | solution.py:262
  25.7 7.5 %collective-permute-start.3 = (bf16[256,2048]{1,0:T(8,128)(2,1)}, bf16[256,2048]{1,0:T(8,128)(2,1)}, u32[]{:S(2)}, u32[]{:S(2)}) collective-permute-start(bf16[256,2048]{1,0:T(8,128)(2,1)} %collective-permute-done.2), channel_id=1, source_target_pairs={{0,1},{1,0},{2,3},{3,2},{4,5},{5,4},{6,7},{7,6},{8,9},{9,8},{10,11... | collective-permute-start | bytes 3145736 | tf_op jit(solution)/shard_map/ppermute | solution.py:22
  31.5 1.7 %copy-start.5 = (bf16[128,2048]{1,0:T(8,128)(2,1)S(1)}, bf16[128,2048]{1,0:T(8,128)(2,1)}, u32[]{:S(2)}) copy-start(bf16[128,2048]{1,0:T(8,128)(2,1)} %param.16) | copy-start | bytes 1572868
  33.2 1.7 %copy-start.32 = (f32[2048]{0:T(1024)S(1)}, f32[2048]{0:T(1024)}, u32[]{:S(2)}) copy-start(f32[2048]{0:T(1024)} %param.18) | copy-start | bytes 24580
  34.9 0.8 copy-start.30
  35.5 7.3 %collective-permute-start.11 = (bf16[64,2048]{1,0:T(8,128)(2,1)S(1)}, bf16[64,2048]{1,0:T(8,128)(2,1)S(1)}, u32[]{:S(2)}, u32[]{:S(2)}) collective-permute-start(bf16[64,2048]{1,0:T(8,128)(2,1)S(1)} %get-tuple-element.7), channel_id=1, source_target_pairs={{0,4},{4,8},{8,12},{12,0},{1,5},{5,9},{9,13},{13,1},{2,6},{6,10},{... | collective-permute-start | bytes 786440 | tf_op jit(solution)/shard_map/ppermute | solution.py:48
  36.1 7.8 %collective-permute-start.7 = (bf16[64,2048]{1,0:T(8,128)(2,1)S(1)}, bf16[64,2048]{1,0:T(8,128)(2,1)S(1)}, u32[]{:S(2)}, u32[]{:S(2)}) collective-permute-start(bf16[64,2048]{1,0:T(8,128)(2,1)S(1)} %concatenate.125), channel_id=1, source_target_pairs={{0,2},{1,3},{2,0},{3,1},{4,6},{5,7},{6,4},{7,5},{8,10},{9,11},{10,... | collective-permute-start | bytes 786440 | tf_op jit(solution)/shard_map/ppermute | solution.py:22
  37.1 20.1 %collective-permute-start.17 = (bf16[64,2048]{1,0:T(8,128)(2,1)S(1)}, bf16[64,2048]{1,0:T(8,128)(2,1)S(1)}, u32[]{:S(2)}, u32[]{:S(2)}) collective-permute-start(bf16[64,2048]{1,0:T(8,128)(2,1)S(1)} %get-tuple-element.9), channel_id=1, source_target_pairs={{0,8},{4,12},{8,0},{12,4},{1,9},{5,13},{9,1},{13,5},{2,10},{6,14},... | collective-permute-start | bytes 786440 | tf_op jit(solution)/shard_map/ppermute | solution.py:48
  38.6 22.2 %collective-permute-start.23 = (bf16[64,2048]{1,0:T(8,128)(2,1)S(1)}, bf16[64,2048]{1,0:T(8,128)(2,1)S(1)}, u32[]{:S(2)}, u32[]{:S(2)}) collective-permute-start(bf16[64,2048]{1,0:T(8,128)(2,1)S(1)} %get-tuple-element.8), channel_id=1, source_target_pairs={{0,12},{4,0},{8,4},{12,8},{1,13},{5,1},{9,5},{13,9},{2,14},{6,2},{... | collective-permute-start | bytes 786440 | tf_op jit(solution)/shard_map/ppermute | solution.py:48
  43.1 20.3 %collective-permute-start.12 = (bf16[64,2048]{1,0:T(8,128)(2,1)S(1)}, bf16[64,2048]{1,0:T(8,128)(2,1)S(1)}, u32[]{:S(2)}, u32[]{:S(2)}) collective-permute-start(bf16[64,2048]{1,0:T(8,128)(2,1)S(1)} %concatenate.127), channel_id=1, source_target_pairs={{0,2},{1,3},{2,0},{3,1},{4,6},{5,7},{6,4},{7,5},{8,10},{9,11},{10,... | collective-permute-start | bytes 786440 | tf_op jit(solution)/shard_map/ppermute | solution.py:22
  43.9 22.1 %copy-start.18 = (bf16[32,2048]{1,0:T(8,128)(2,1)}, bf16[32,2048]{1,0:T(8,128)(2,1)S(1)}, u32[]{:S(2)}) copy-start(bf16[32,2048]{1,0:T(8,128)(2,1)S(1)} %get-tuple-element.42) | copy-start | bytes 393220
  43.9 22.0 %collective-permute-start.8 = (bf16[64,2048]{1,0:T(8,128)(2,1)S(1)}, bf16[64,2048]{1,0:T(8,128)(2,1)S(1)}, u32[]{:S(2)}, u32[]{:S(2)}) collective-permute-start(bf16[64,2048]{1,0:T(8,128)(2,1)S(1)} %pad_maximum_fusion.8), channel_id=1, source_target_pairs={{0,1},{1,0},{2,3},{3,2},{4,5},{5,4},{6,7},{7,6},{8,9},{9,8},{10,11... | collective-permute-start | bytes 786440 | tf_op jit(solution)/shard_map/ppermute | solution.py:22
  58.3 8.3 %copy-start.35 = (bf16[1,2048,512]{2,1,0:T(8,128)(2,1)S(1)}, bf16[1,2048,512]{2,1,0:T(8,128)(2,1)}, u32[]{:S(2)}) copy-start(bf16[1,2048,512]{2,1,0:T(8,128)(2,1)} %param.20) | copy-start | bytes 6291460
  58.3 15.6 %collective-permute-start.18 = (bf16[64,2048]{1,0:T(8,128)(2,1)}, bf16[64,2048]{1,0:T(8,128)(2,1)}, u32[]{:S(2)}, u32[]{:S(2)}) collective-permute-start(bf16[64,2048]{1,0:T(8,128)(2,1)} %concatenate.129), channel_id=1, source_target_pairs={{0,2},{1,3},{2,0},{3,1},{4,6},{5,7},{6,4},{7,5},{8,10},{9,11},{10,... | collective-permute-start | bytes 786440 | tf_op jit(solution)/shard_map/ppermute | solution.py:22
  61.8 14.8 %collective-permute-start.24 = (bf16[64,2048]{1,0:T(8,128)(2,1)}, bf16[64,2048]{1,0:T(8,128)(2,1)}, u32[]{:S(2)}, u32[]{:S(2)}) collective-permute-start(bf16[64,2048]{1,0:T(8,128)(2,1)} %concatenate.131), channel_id=1, source_target_pairs={{0,2},{1,3},{2,0},{3,1},{4,6},{5,7},{6,4},{7,5},{8,10},{9,11},{10,... | collective-permute-start | bytes 786440 | tf_op jit(solution)/shard_map/ppermute | solution.py:22
  64.8 14.3 %collective-permute-start.13 = (bf16[64,2048]{1,0:T(8,128)(2,1)}, bf16[64,2048]{1,0:T(8,128)(2,1)}, u32[]{:S(2)}, u32[]{:S(2)}) collective-permute-start(bf16[64,2048]{1,0:T(8,128)(2,1)} %pad_maximum_fusion.10), channel_id=1, source_target_pairs={{0,1},{1,0},{2,3},{3,2},{4,5},{5,4},{6,7},{7,6},{8,9},{9,8},{10,11... | collective-permute-start | bytes 786440 | tf_op jit(solution)/shard_map/ppermute | solution.py:22
  65.9 0.7 copy-start.22
  71.2 7.9 %copy-start.3 = (bf16[128,2048]{1,0:T(8,128)(2,1)S(1)}, bf16[128,2048]{1,0:T(8,128)(2,1)}, u32[]{:S(2)}) copy-start(bf16[128,2048]{1,0:T(8,128)(2,1)} %convolution_convert_fusion.7) | copy-start | bytes 1572868
  71.2 9.7 %copy-start.12 = (bf16[32,2048]{1,0:T(8,128)(2,1)S(1)}, bf16[32,2048]{1,0:T(8,128)(2,1)}, u32[]{:S(2)}) copy-start(bf16[32,2048]{1,0:T(8,128)(2,1)} %get-tuple-element.14) | copy-start | bytes 393220
  71.2 9.7 %copy-start.17 = (bf16[32,2048]{1,0:T(8,128)(2,1)S(1)}, bf16[32,2048]{1,0:T(8,128)(2,1)}, u32[]{:S(2)}) copy-start(bf16[32,2048]{1,0:T(8,128)(2,1)} %get-tuple-element.34) | copy-start | bytes 393220
  71.2 9.7 %copy-start.36 = (bf16[1,2048,512]{2,1,0:T(8,128)(2,1)S(1)}, bf16[1,2048,512]{2,1,0:T(8,128)(2,1)}, u32[]{:S(2)}) copy-start(bf16[1,2048,512]{2,1,0:T(8,128)(2,1)} %param.20) | copy-start | bytes 6291460
  73.1 14.9 %collective-permute-start.9 = (bf16[64,2048]{1,0:T(8,128)(2,1)}, bf16[64,2048]{1,0:T(8,128)(2,1)}, u32[]{:S(2)}, u32[]{:S(2)}) collective-permute-start(bf16[64,2048]{1,0:T(8,128)(2,1)} %concatenate.126), channel_id=1, source_target_pairs={{0,2},{1,3},{2,0},{3,1},{4,6},{5,7},{6,4},{7,5},{8,10},{9,11},{10,... | collective-permute-start | bytes 786440 | tf_op jit(solution)/shard_map/ppermute | solution.py:22
  76.3 15.6 %collective-permute-start.19 = (bf16[64,2048]{1,0:T(8,128)(2,1)}, bf16[64,2048]{1,0:T(8,128)(2,1)}, u32[]{:S(2)}, u32[]{:S(2)}) collective-permute-start(bf16[64,2048]{1,0:T(8,128)(2,1)} %pad_maximum_fusion.12), channel_id=1, source_target_pairs={{0,1},{1,0},{2,3},{3,2},{4,5},{5,4},{6,7},{7,6},{8,9},{9,8},{10,11... | collective-permute-start | bytes 786440 | tf_op jit(solution)/shard_map/ppermute | solution.py:22
  78.9 23.6 %collective-permute-start.25 = (bf16[64,2048]{1,0:T(8,128)(2,1)}, bf16[64,2048]{1,0:T(8,128)(2,1)}, u32[]{:S(2)}, u32[]{:S(2)}) collective-permute-start(bf16[64,2048]{1,0:T(8,128)(2,1)} %pad_maximum_fusion.14), channel_id=1, source_target_pairs={{0,1},{1,0},{2,3},{3,2},{4,5},{5,4},{6,7},{7,6},{8,9},{9,8},{10,11... | collective-permute-start | bytes 786440 | tf_op jit(solution)/shard_map/ppermute | solution.py:22
  79.1 2.9 %copy-start.13 = (bf16[32,2048]{1,0:T(8,128)(2,1)S(1)}, bf16[32,2048]{1,0:T(8,128)(2,1)}, u32[]{:S(2)}) copy-start(bf16[32,2048]{1,0:T(8,128)(2,1)} %get-tuple-element.14) | copy-start | bytes 393220
  80.2 0.7 copy-start.24
  85.5 8.1 %copy-start.10 = (bf16[32,2048]{1,0:T(8,128)(2,1)S(1)}, bf16[32,2048]{1,0:T(8,128)(2,1)}, u32[]{:S(2)}) copy-start(bf16[32,2048]{1,0:T(8,128)(2,1)} %get-tuple-element.22) | copy-start | bytes 393220
  85.5 8.1 %copy-start.16 = (bf16[32,2048]{1,0:T(8,128)(2,1)S(1)}, bf16[32,2048]{1,0:T(8,128)(2,1)}, u32[]{:S(2)}) copy-start(bf16[32,2048]{1,0:T(8,128)(2,1)} %get-tuple-element.50) | copy-start | bytes 393220
  85.5 8.1 %copy-start.37 = (bf16[1,2048,512]{2,1,0:T(8,128)(2,1)S(1)}, bf16[1,2048,512]{2,1,0:T(8,128)(2,1)}, u32[]{:S(2)}) copy-start(bf16[1,2048,512]{2,1,0:T(8,128)(2,1)} %param.20) | copy-start | bytes 6291460
  87.3 26.7 %collective-permute-start.14 = (bf16[64,2048]{1,0:T(8,128)(2,1)}, bf16[64,2048]{1,0:T(8,128)(2,1)}, u32[]{:S(2)}, u32[]{:S(2)}) collective-permute-start(bf16[64,2048]{1,0:T(8,128)(2,1)} %concatenate.128), channel_id=1, source_target_pairs={{0,2},{1,3},{2,0},{3,1},{4,6},{5,7},{6,4},{7,5},{8,10},{9,11},{10,... | collective-permute-start | bytes 786440 | tf_op jit(solution)/shard_map/ppermute | solution.py:22
  89.7 32.2 %collective-permute-start.10 = (bf16[64,2048]{1,0:T(8,128)(2,1)}, bf16[64,2048]{1,0:T(8,128)(2,1)}, u32[]{:S(2)}, u32[]{:S(2)}) collective-permute-start(bf16[64,2048]{1,0:T(8,128)(2,1)} %pad_maximum_fusion.9), channel_id=1, source_target_pairs={{0,1},{1,0},{2,3},{3,2},{4,5},{5,4},{6,7},{7,6},{8,9},{9,8},{10,11... | collective-permute-start | bytes 786440 | tf_op jit(solution)/shard_map/ppermute | solution.py:22
  92.9 0.7 copy-start.26
  100.0 16.9 %collective-permute-start.20 = (bf16[64,2048]{1,0:T(8,128)(2,1)}, bf16[64,2048]{1,0:T(8,128)(2,1)}, u32[]{:S(2)}, u32[]{:S(2)}) collective-permute-start(bf16[64,2048]{1,0:T(8,128)(2,1)} %concatenate.130), channel_id=1, source_target_pairs={{0,2},{1,3},{2,0},{3,1},{4,6},{5,7},{6,4},{7,5},{8,10},{9,11},{10,... | collective-permute-start | bytes 786440 | tf_op jit(solution)/shard_map/ppermute | solution.py:22
  103.5 0.7 copy-start.28
  110.7 7.9 %copy-start.6 = (bf16[32,2048]{1,0:T(8,128)(2,1)S(1)}, bf16[32,2048]{1,0:T(8,128)(2,1)}, u32[]{:S(2)}) copy-start(bf16[32,2048]{1,0:T(8,128)(2,1)} %get-tuple-element.21) | copy-start | bytes 393220
  111.7 7.6 %collective-permute-start.26 = (bf16[64,2048]{1,0:T(8,128)(2,1)S(1)}, bf16[64,2048]{1,0:T(8,128)(2,1)S(1)}, u32[]{:S(2)}, u32[]{:S(2)}) collective-permute-start(bf16[64,2048]{1,0:T(8,128)(2,1)S(1)} %concatenate.132), channel_id=1, source_target_pairs={{0,2},{1,3},{2,0},{3,1},{4,6},{5,7},{6,4},{7,5},{8,10},{9,11},{10,... | collective-permute-start | bytes 786440 | tf_op jit(solution)/shard_map/ppermute | solution.py:22
  116.4 18.8 %collective-permute-start.15 = (bf16[64,2048]{1,0:T(8,128)(2,1)}, bf16[64,2048]{1,0:T(8,128)(2,1)}, u32[]{:S(2)}, u32[]{:S(2)}) collective-permute-start(bf16[64,2048]{1,0:T(8,128)(2,1)} %pad_maximum_fusion.11), channel_id=1, source_target_pairs={{0,1},{1,0},{2,3},{3,2},{4,5},{5,4},{6,7},{7,6},{8,9},{9,8},{10,11... | collective-permute-start | bytes 786440 | tf_op jit(solution)/shard_map/ppermute | solution.py:22
  119.3 8.5 %collective-permute-start.21 = (bf16[64,2048]{1,0:T(8,128)(2,1)}, bf16[64,2048]{1,0:T(8,128)(2,1)}, u32[]{:S(2)}, u32[]{:S(2)}) collective-permute-start(bf16[64,2048]{1,0:T(8,128)(2,1)} %pad_maximum_fusion.13), channel_id=1, source_target_pairs={{0,1},{1,0},{2,3},{3,2},{4,5},{5,4},{6,7},{7,6},{8,9},{9,8},{10,11... | collective-permute-start | bytes 786440 | tf_op jit(solution)/shard_map/ppermute | solution.py:22
  120.7 12.8 %collective-permute-start.27 = (bf16[64,2048]{1,0:T(8,128)(2,1)}, bf16[64,2048]{1,0:T(8,128)(2,1)}, u32[]{:S(2)}, u32[]{:S(2)}) collective-permute-start(bf16[64,2048]{1,0:T(8,128)(2,1)} %pad_maximum_fusion.15), channel_id=1, source_target_pairs={{0,1},{1,0},{2,3},{3,2},{4,5},{5,4},{6,7},{7,6},{8,9},{9,8},{10,11... | collective-permute-start | bytes 786440 | tf_op jit(solution)/shard_map/ppermute | solution.py:22
  127.8 2.3 %copy-start.14 = (bf16[32,2048]{1,0:T(8,128)(2,1)S(1)}, bf16[32,2048]{1,0:T(8,128)(2,1)}, u32[]{:S(2)}) copy-start(bf16[32,2048]{1,0:T(8,128)(2,1)} %get-tuple-element.20) | copy-start | bytes 393220
  127.8 2.3 %copy-start.20 = (bf16[32,2048]{1,0:T(8,128)(2,1)S(1)}, bf16[32,2048]{1,0:T(8,128)(2,1)}, u32[]{:S(2)}) copy-start(bf16[32,2048]{1,0:T(8,128)(2,1)} %get-tuple-element.46) | copy-start | bytes 393220
  127.8 2.3 %copy-start.29 = (bf16[4,64,128]{2,1,0:T(8,128)(2,1)S(1)}, bf16[4,64,128]{2,1,0:T(8,128)(2,1)}, u32[]{:S(2)}) copy-start(bf16[4,64,128]{2,1,0:T(8,128)(2,1)} %get-tuple-element.6) | copy-start | bytes 196612
  128.9 5.7 %copy-start.15 = (bf16[32,2048]{1,0:T(8,128)(2,1)S(1)}, bf16[32,2048]{1,0:T(8,128)(2,1)}, u32[]{:S(2)}) copy-start(bf16[32,2048]{1,0:T(8,128)(2,1)} %get-tuple-element.24) | copy-start | bytes 393220
  128.9 5.7 %copy-start.19 = (bf16[32,2048]{1,0:T(8,128)(2,1)S(1)}, bf16[32,2048]{1,0:T(8,128)(2,1)}, u32[]{:S(2)}) copy-start(bf16[32,2048]{1,0:T(8,128)(2,1)} %get-tuple-element.54) | copy-start | bytes 393220
  128.9 5.7 %copy-start.31 = (bf16[4,64,128]{2,1,0:T(8,128)(2,1)S(1)}, bf16[4,64,128]{2,1,0:T(8,128)(2,1)}, u32[]{:S(2)}) copy-start(bf16[4,64,128]{2,1,0:T(8,128)(2,1)} %get-tuple-element.5) | copy-start | bytes 196612
  130.4 12.7 %collective-permute-start.22 = (bf16[64,2048]{1,0:T(8,128)(2,1)S(1)}, bf16[64,2048]{1,0:T(8,128)(2,1)S(1)}, u32[]{:S(2)}, u32[]{:S(2)}) collective-permute-start(bf16[64,2048]{1,0:T(8,128)(2,1)S(1)} %fusion.8), channel_id=1, source_target_pairs={{0,8},{4,12},{8,0},{12,4},{1,9},{5,13},{9,1},{13,5},{2,10},{6,14},... | collective-permute-start | bytes 786440 | tf_op jit(solution)/shard_map/ppermute | solution.py:48
  134.6 1.5 copy-start.9
  134.6 1.5 copy-start.11
  135.0 8.0 %copy-start.8 = (pred[256,128]{1,0:T(32,128)(4,1)S(1)}, pred[256,128]{1,0:T(32,128)(4,1)}, u32[]{:S(2)}) copy-start(pred[256,128]{1,0:T(32,128)(4,1)} %iota_compare_fusion.2) | copy-start | bytes 98308
  135.0 19.3 %collective-permute-start.28 = (bf16[64,2048]{1,0:T(8,128)(2,1)S(1)}, bf16[64,2048]{1,0:T(8,128)(2,1)S(1)}, u32[]{:S(2)}, u32[]{:S(2)}) collective-permute-start(bf16[64,2048]{1,0:T(8,128)(2,1)S(1)} %fusion.9), channel_id=1, source_target_pairs={{0,4},{4,8},{8,12},{12,0},{1,5},{5,9},{9,13},{13,1},{2,6},{6,10},{... | collective-permute-start | bytes 786440 | tf_op jit(solution)/shard_map/ppermute | solution.py:48
  136.4 18.4 %copy-start.1 = (f32[128,2048]{1,0:T(8,128)S(1)}, f32[128,2048]{1,0:T(8,128)}, u32[]{:S(2)}) copy-start(f32[128,2048]{1,0:T(8,128)} %convolution_add_fusion.1) | copy-start | bytes 3145732
  136.6 18.1 %collective-permute-start.16 = (bf16[64,2048]{1,0:T(8,128)(2,1)S(1)}, bf16[64,2048]{1,0:T(8,128)(2,1)S(1)}, u32[]{:S(2)}, u32[]{:S(2)}) collective-permute-start(bf16[64,2048]{1,0:T(8,128)(2,1)S(1)} %fusion.7), channel_id=1, source_target_pairs={{0,12},{4,0},{8,4},{12,8},{1,13},{5,1},{9,5},{13,9},{2,14},{6,2},{... | collective-permute-start | bytes 786440 | tf_op jit(solution)/shard_map/ppermute | solution.py:48
  (5 other events, 3.2 us)
